TPU v7x, 32 devices: a whole 2x2x4 slice. The times are simulated.
32 devices in a mesh: sp: 8 (over z, x), tp: 4 (over y, core).
Axes of the slice: x: 2, y: 2, z: 4, core: 2. Of those that a mesh axis runs over, the one named last changes fastest.
Arguments:
- conv_value: bfloat16 [4096, 1024], P('sp', 'tp'), may hold values from -6 to 6
- conv_gate: bfloat16 [4096, 1024], P('sp', 'tp'), may hold values from -9 to 9
- conv_weight: float32 [31, 1024], P(None, 'tp'), may hold values from -2.2 to 2.2
- conv_gain: float32 [1024], P('tp'), may hold values from 0.1 to 1.9
- conv_shift: float32 [1024], P('tp'), may hold values from -3 to 3
- out_weight: bfloat16 [1024, 2048], P('tp'), may hold values from -0.1875 to 0.1875
- residual: bfloat16 [4096, 2048], P('sp', 'tp'), may hold values from -10 to 10
- mix_gain: float32 [2048], P('tp'), may hold values from 0.1 to 1.9
- expert_ids: int32 [4096, 2], P('sp'), may hold values from 0 to 7, all different within a row; in each aligned block of 128 rows (0 to 127, 128 to 255, ...) at most 64 rows name the same one
- group_weight: float32 [4096], P('sp'), may hold values from 0.6 to 1
- score_gap: float32 [4096], P('sp'), may hold values from -0.8 to 0.8
- w_gate: bfloat16 [8, 2048, 1024], P('sp', None, 'tp'), may hold values from -0.125 to 0.125
- w_up: bfloat16 [8, 2048, 1024], P('sp', None, 'tp'), may hold values from -0.125 to 0.125
- w_down: bfloat16 [8, 1024, 2048], P('sp', 'tp'), may hold values from -0.1875 to 0.1875
Outputs:
- layer_out: bfloat16 [4096, 2048], P('sp', 'tp')
Inputs may be any that keep to these rules, and one draw needn't show every extreme that they name: `expert_ids`: the two experts of a position differ. In each aligned block of 512 // 4 positions no expert is named by more than 64 rows, a bound that some block reaches.
All inputs are finite; a program needn't handle non-finite values.
Results may differ from a plain program's by a relative error of at most 0.012.
Values may be sent and summed in bfloat16 or wider, within the bound.
No kernel may reach another device: no remote copies, remote signals or barrier semaphores. Data moves between devices by JAX's collectives and lax.ppermute only.
A program may use at most 128 MiB of HBM per device.

v0:
```python
import jax
import jax.numpy as jnp
from jax import lax
from jax.experimental import pallas as pl
from jax.experimental.pallas import tpu as pltpu
from jax.sharding import Mesh
from jax.sharding import PartitionSpec as P


D = 2048
CH = 1024


eps = 1e-06
FEW = 8


def swap(value, bit):
    count = lax.axis_size("tp")
    return lax.ppermute(value, "tp", [(source, source ^ bit) for source in range(count)])


def natural(blocks, index):
    ordered = []
    for place in range(len(blocks)):
        chosen = blocks[0]
        for bit in range(1, len(blocks)):
            chosen = jnp.where(index == (place ^ bit), blocks[bit], chosen)
        ordered.append(chosen)
    return ordered


def exchanged(piece):
    count = lax.axis_size("tp")
    blocks = [piece(0)]
    for bit in range(1, count):
        blocks.append(swap(piece(bit), bit))
    return blocks


def gathered(block):
    count = lax.axis_size("tp")
    held = {0: block}
    bit = count // 2
    while bit:
        for have in sorted(held):
            held[bit ^ have] = swap(held[have], bit)
        bit //= 2
    return [held[bit] for bit in range(count)]


def dot(left, right):
    return jnp.dot(left, right, preferred_element_type=jnp.float32)


def hidden_kernel(places, blocks, *refs):
    pieces = max(len(places), 1)
    x_refs, refs = refs[:pieces], refs[pieces:]
    weight_refs, refs = refs[: 2 * blocks], refs[2 * blocks :]
    own_ref, other_ref, refs = refs[0], refs[1], refs[2:]
    x, (held, sems) = (refs[0], refs[1:]) if places else (x_refs[0], refs)
    width = weight_refs[0].shape[1]
    copies = [
        pltpu.make_async_copy(ref, held.at[i // 2, :, pl.ds(i % 2 * width, width)], sems.at[i])
        for i, ref in enumerate(weight_refs)
    ]
    for copy in copies:
        copy.start()
    for (top, left), x_ref in zip(places, x_refs):
        height, columns = x_ref.shape
        x[top : top + height, left : left + columns] = x_ref[...]
    half = own_ref.shape[0]
    for block in range(blocks):
        copies[2 * block].wait()
        copies[2 * block + 1].wait()
        for i, out_ref in enumerate((own_ref, other_ref)):
            both = dot(x[i * half : (i + 1) * half], held[block])
            gate, up = both[:, :width], both[:, width:]
            out_ref[:, block * width : (block + 1) * width] = (jax.nn.silu(gate) * up).astype(
                jnp.bfloat16
            )


def whole(shape):
    return pl.BlockSpec(shape, lambda i: (0,) * len(shape))


def hidden_rows(pieces, places, rows, gates, ups):
    depth, width = gates[0].shape
    blocks = len(gates)
    weights = [w for pair in zip(gates, ups) for w in pair]
    hidden = (rows // 2, blocks * width)
    outs = [hidden, hidden] + [(rows, depth)] * bool(places)
    return pl.pallas_call(
        lambda *refs: hidden_kernel(places, blocks, *refs),
        out_shape=[jax.ShapeDtypeStruct(out, jnp.bfloat16) for out in outs],
        grid=(1,),
        in_specs=[whole(piece.shape) for piece in pieces]
        + [pl.BlockSpec(memory_space=pltpu.HBM)] * (2 * blocks),
        out_specs=[whole(out) for out in outs],
        scratch_shapes=[
            pltpu.VMEM((blocks, depth, 2 * width), jnp.bfloat16),
            pltpu.SemaphoreType.DMA((2 * blocks,)),
        ],
        compiler_params=pltpu.CompilerParams(vmem_limit_bytes=24 << 20),
        cost_estimate=pl.CostEstimate(
            flops=4 * blocks * rows * depth * width,
            bytes_accessed=2 * (rows * depth + blocks * width * (2 * depth + rows)),
            transcendentals=blocks * rows * width,
        ),
        name="hidden",
    )(*pieces, *weights)


def down_kernel(parts, blocks, *refs):
    hidden_refs, refs = refs[:parts], refs[parts:]
    down_refs, out_refs = refs[:blocks], refs[blocks:]
    width = down_refs[0].shape[0]
    total, block = 0.0, 0
    for hidden_ref in hidden_refs:
        for low in range(0, hidden_ref.shape[1], width):
            total = total + dot(hidden_ref[:, low : low + width], down_refs[block][...])
            block += 1
    height = out_refs[0].shape[0]
    for i, out_ref in enumerate(out_refs):
        out_ref[...] = total[i * height : (i + 1) * height].astype(jnp.bfloat16)


def down_rows(hiddens, downs, pieces):
    rows = hiddens[0].shape[0]
    width, columns = downs[0].shape
    blocks = len(downs)
    depth = blocks * width
    tile = min(columns, 512)
    height = rows // pieces
    return pl.pallas_call(
        lambda *refs: down_kernel(len(hiddens), blocks, *refs),
        out_shape=[jax.ShapeDtypeStruct((height, columns), jnp.bfloat16)] * pieces,
        grid=(columns // tile,),
        in_specs=[whole(hidden.shape) for hidden in hiddens]
        + [pl.BlockSpec((width, tile), lambda i: (0, i))] * blocks,
        out_specs=[pl.BlockSpec((height, tile), lambda i: (0, i))] * pieces,
        compiler_params=pltpu.CompilerParams(vmem_limit_bytes=20 << 20),
        cost_estimate=pl.CostEstimate(
            flops=2 * rows * depth * columns,
            bytes_accessed=2 * (rows * depth + depth * columns + rows * columns),
            transcendentals=0,
        ),
        name="down",
    )(*hiddens, *downs)


def placed_kernel(parts, pick_ref, *refs):
    rows_refs, out_refs = refs[:parts], refs[parts:]
    height = out_refs[0].shape[0]
    low = 0
    for rows_ref in rows_refs:
        high = low + rows_ref.shape[1]
        for i, out_ref in enumerate(out_refs):
            pick = pick_ref[i * height : (i + 1) * height]
            out_ref[:, low:high] = dot(pick, rows_ref[...]).astype(jnp.bfloat16)
        low = high


def placed(pick, parts, pieces):
    count = parts[0].shape[0]
    columns = sum(part.shape[1] for part in parts)
    height = pick.shape[0] // pieces
    return pl.pallas_call(
        lambda *refs: placed_kernel(len(parts), *refs),
        out_shape=[jax.ShapeDtypeStruct((height, columns), jnp.bfloat16)] * pieces,
        grid=(1,),
        in_specs=[whole(value.shape) for value in (pick, *parts)],
        out_specs=[whole((height, columns))] * pieces,
        compiler_params=pltpu.CompilerParams(vmem_limit_bytes=16 << 20),
        cost_estimate=pl.CostEstimate(
            flops=2 * pick.shape[0] * count * columns,
            bytes_accessed=2 * (pick.shape[0] + count) * columns,
            transcendentals=0,
        ),
        name="placed",
    )(pick, *parts)


def across_slots(pick, held):
    return lax.dot_general(pick, held, (((0,), (0,)), ((), ())), preferred_element_type=jnp.float32)


def weighted_kernel(pieces, high_ref, low_ref, *refs):
    block_refs, add_refs, (out_ref, held, added, sems) = refs[:pieces], refs[pieces:-4], refs[-4:]
    height = block_refs[0].shape[0]
    copies = [
        pltpu.make_async_copy(ref, held.at[pl.ds(i * height, height), :], sems.at[i])
        for i, ref in enumerate(block_refs)
    ]
    for i, ref in enumerate(add_refs):
        copies.append(pltpu.make_async_copy(ref, added.at[i], sems.at[pieces + i]))
    for copy in copies:
        copy.start()
    for copy in copies:
        copy.wait()
    total = across_slots(high_ref[...], held[...]) + across_slots(low_ref[...], held[...])
    for i in range(len(add_refs)):
        total = total + added[i].astype(jnp.float32)
    out_ref[...] = total.astype(jnp.bfloat16)


def weighted(gates, blocks, adds=()):
    rows = gates[0].shape[1]
    height, columns = blocks[0].shape
    pieces = len(blocks)
    return pl.pallas_call(
        lambda *refs: weighted_kernel(pieces, *refs),
        out_shape=jax.ShapeDtypeStruct((rows, columns), jnp.bfloat16),
        grid=(1,),
        in_specs=[whole(value.shape) for value in gates]
        + [pl.BlockSpec(memory_space=pltpu.HBM)] * (pieces + len(adds)),
        out_specs=whole((rows, columns)),
        scratch_shapes=[
            pltpu.VMEM((pieces * height, columns), jnp.bfloat16),
            pltpu.VMEM((max(len(adds), 1), rows, columns), jnp.bfloat16),
            pltpu.SemaphoreType.DMA((pieces + len(adds),)),
        ],
        compiler_params=pltpu.CompilerParams(vmem_limit_bytes=16 << 20),
        cost_estimate=pl.CostEstimate(
            flops=4 * pieces * height * rows * columns,
            bytes_accessed=2 * (pieces * height + rows) * columns,
            transcendentals=0,
        ),
        name="weighted",
    )(*gates, *blocks, *adds)


def route_kernel(experts, capacity, where_ref, about_ref, place_ref, high_ref, low_ref):
    low, order = where_ref[0], where_ref[1]
    rows = about_ref.shape[1]
    first = about_ref[0:1, :].astype(jnp.int32) - low
    second = about_ref[1:2, :].astype(jnp.int32) - low
    height = max(experts, 8)
    named = lax.broadcasted_iota(jnp.int32, (height, rows), 0)
    first_hot = (named == first).astype(jnp.float32)
    second_hot = (named == second).astype(jnp.float32)
    down = lax.broadcasted_iota(jnp.int32, (rows, rows), 0)
    right = lax.broadcasted_iota(jnp.int32, (rows, rows), 1)
    earlier = (down < right).astype(jnp.float32).astype(jnp.bfloat16)
    before = dot((first_hot + second_hot).astype(jnp.bfloat16), earlier)
    slot = lax.broadcasted_iota(jnp.int32, (experts * capacity, rows), 0)
    weight, gap = about_ref[2:3, :], about_ref[3:4, :]
    place, gates = 0.0, 0.0
    for ids, hot, gate in (
        (first, first_hot, weight * jax.nn.sigmoid(gap)),
        (second, second_hot, weight * jax.nn.sigmoid(-gap)),
    ):
        rank = jnp.sum(before * hot, axis=0, keepdims=True).astype(jnp.int32)
        here = (ids >= 0) & (ids < experts)
        mine = jnp.where(here, (ids ^ order) * capacity + rank, -1)
        pick = (slot == mine).astype(jnp.float32)
        place = place + pick
        gates = gates + pick * gate
    place_ref[...] = place.astype(jnp.bfloat16)
    high = gates.astype(jnp.bfloat16)
    high_ref[...] = high
    low_ref[...] = (gates - high.astype(jnp.float32)).astype(jnp.bfloat16)


def routing(about, experts, capacity, low, order):
    shape = (experts * capacity, about.shape[1])
    where = jnp.stack([low, order]).astype(jnp.int32)
    return pl.pallas_call(
        lambda *refs: route_kernel(experts, capacity, *refs),
        out_shape=[jax.ShapeDtypeStruct(shape, jnp.bfloat16)] * 3,
        grid_spec=pltpu.PrefetchScalarGridSpec(
            num_scalar_prefetch=1,
            grid=(1,),
            in_specs=[pl.BlockSpec(about.shape, lambda i, where: (0, 0))],
            out_specs=[pl.BlockSpec(shape, lambda i, where: (0, 0))] * 3,
        ),
        compiler_params=pltpu.CompilerParams(vmem_limit_bytes=8 << 20),
        cost_estimate=pl.CostEstimate(
            flops=40 * shape[0] * shape[1], bytes_accessed=6 * shape[0] * shape[1], transcendentals=0
        ),
        name="route",
    )(where, about)


def conv_kernel(blocks, taps, halo, *refs):
    window_refs, small_refs, refs = refs[:blocks], refs[blocks : 2 * blocks], refs[2 * blocks :]
    out_ref, gains_ref, wide, held = refs
    rows, width = out_ref.shape[0], window_refs[0].shape[1]
    row_sum, row_sq = 0.0, 0.0
    for block in range(blocks):
        wide[...] = window_refs[block][...].astype(jnp.float32)
        total = jnp.zeros((rows, width), jnp.float32)
        for tap in range(taps):
            start = halo - taps + 1 + tap
            total = total + small_refs[block][tap : tap + 1, :] * wide[start : start + rows, :]
        held[block] = total
        row_sum = row_sum + jnp.sum(total, axis=-1, keepdims=True)
        row_sq = row_sq + jnp.sum(total * total, axis=-1, keepdims=True)
        gains = small_refs[block][taps + 2 :, :]
        gains_ref[block * gains.shape[0] : (block + 1) * gains.shape[0], :] = gains
    mean = row_sum / CH
    scale = lax.rsqrt(row_sq / CH - mean * mean + eps)
    for block in range(blocks):
        gain, shift = small_refs[block][taps : taps + 1, :], small_refs[block][taps + 1 : taps + 2, :]
        normalized = (held[block] - mean) * scale * gain + shift
        out_ref[:, block * width : (block + 1) * width] = jax.nn.silu(normalized).astype(jnp.bfloat16)


def conv_rows(windows, smalls, taps):
    high, width = windows[0].shape
    halo = -(-(taps - 1) // 16) * 16
    rows, blocks = high - halo, len(windows)
    gains = (blocks * (smalls[0].shape[0] - taps - 2), width)
    return pl.pallas_call(
        lambda *refs: conv_kernel(blocks, taps, halo, *refs),
        out_shape=[
            jax.ShapeDtypeStruct((rows, blocks * width), jnp.bfloat16),
            jax.ShapeDtypeStruct(gains, jnp.float32),
        ],
        grid=(1,),
        in_specs=[whole(value.shape) for value in (*windows, *smalls)],
        out_specs=[whole((rows, blocks * width)), whole(gains)],
        scratch_shapes=[
            pltpu.VMEM((high, width), jnp.float32),
            pltpu.VMEM((blocks, rows, width), jnp.float32),
        ],
        compiler_params=pltpu.CompilerParams(vmem_limit_bytes=16 << 20),
        cost_estimate=pl.CostEstimate(
            flops=2 * taps * rows * blocks * width,
            bytes_accessed=4 * blocks * high * width,
            transcendentals=blocks * rows * width,
        ),
        name="conv",
    )(*windows, *smalls)


def near_kernel(blocks, act_ref, *refs):
    weight_refs, out_ref = refs[:blocks], refs[blocks]
    width = weight_refs[0].shape[0]
    total = 0.0
    for block, ref in enumerate(weight_refs):
        total = total + dot(act_ref[:, block * width : (block + 1) * width], ref[...])
    out_ref[...] = total


def near_product(act, weights):
    rows = act.shape[0]
    width, columns = weights[0].shape
    tile = min(columns, 1024)
    return pl.pallas_call(
        lambda *refs: near_kernel(len(weights), *refs),
        out_shape=jax.ShapeDtypeStruct((rows, columns), jnp.float32),
        grid=(columns // tile,),
        in_specs=[whole(act.shape)] + [pl.BlockSpec((width, tile), lambda i: (0, i))] * len(weights),
        out_specs=pl.BlockSpec((rows, tile), lambda i: (0, i)),
        compiler_params=pltpu.CompilerParams(vmem_limit_bytes=16 << 20),
        cost_estimate=pl.CostEstimate(
            flops=2 * rows * width * columns * len(weights),
            bytes_accessed=2 * width * columns * len(weights),
            transcendentals=0,
        ),
        name="near_product",
    )(act, *weights)


def middle_kernel(blocks, first, share, where_ref, act_ref, near_ref, gains_ref, *refs):
    count = share * (blocks - first)
    part_refs, residual_refs, refs = refs[:count], refs[count : count + blocks], refs[count + blocks :]
    middle_refs, normed_refs, (total, held, gains, sems) = refs[:2], refs[2:4], refs[4:]
    tp, share_at = where_ref[0], where_ref[1]
    part, columns = part_refs[0].shape
    width = share * part
    copies = []
    for i, ref in enumerate(part_refs):
        row = pl.multiple_of(i // share * width + (share_at ^ (i % share)) * part, part)
        copies.append(pltpu.make_async_copy(ref, held.at[pl.ds(row, part), :], sems.at[i]))
    for copy in copies:
        copy.start()
    for block in range(blocks - first):
        for copy in copies[block * share : (block + 1) * share]:
            copy.wait()
        low = (first + block) * width
        product = dot(act_ref[:, low : low + width], held[block * width : (block + 1) * width])
        total[...] = (total if block else near_ref)[...] + product
    narrow = middle_refs[0].shape[1] // blocks
    row_sq = 0.0
    for block in range(blocks):
        at = tp ^ block
        for k in (0, 1):
            here = pl.ds(pl.multiple_of((2 * at + k) * narrow, narrow), narrow)
            there = pl.ds(pl.multiple_of(at * narrow, narrow), narrow)
            wide = residual_refs[block][:, k * narrow : (k + 1) * narrow].astype(jnp.float32)
            rounded = (wide + total[:, here]).astype(jnp.bfloat16)
            middle_refs[k][:, there] = rounded
            wide = rounded.astype(jnp.float32)
            total[:, here] = wide
            row_sq = row_sq + jnp.sum(wide * wide, axis=-1, keepdims=True)
            for g in range(0, narrow, width):
                line = (2 * block + k) * narrow // width + g // width
                lane = pl.multiple_of((2 * at + k) * narrow + g, width)
                gains[:, pl.ds(lane, width)] = gains_ref[line : line + 1, :]
    scale = lax.rsqrt(row_sq / D + eps)
    half = columns // 2
    for i, ref in enumerate(normed_refs):
        here = slice(i * half, (i + 1) * half)
        ref[...] = (total[:, here] * scale * gains[:, here]).astype(jnp.bfloat16)


def middle_rows(act, near, gains, far_blocks, residuals, where):
    rows, columns = near.shape
    blocks = len(residuals)
    first = blocks - len(far_blocks)
    share = len(far_blocks[0])
    parts = [piece for block in far_blocks for piece in block]
    part = parts[0].shape[0]
    half = (rows, columns // 2)
    spec = lambda shape: pl.BlockSpec(shape, lambda i, where: (0,) * len(shape))
    ins = [act, near, gains]
    return pl.pallas_call(
        lambda *refs: middle_kernel(blocks, first, share, *refs),
        out_shape=[jax.ShapeDtypeStruct(half, jnp.bfloat16)] * 4,
        grid_spec=pltpu.PrefetchScalarGridSpec(
            num_scalar_prefetch=1,
            grid=(1,),
            in_specs=[spec(v.shape) for v in ins]
            + [pl.BlockSpec(memory_space=pl.ANY)] * len(parts)
            + [spec(v.shape) for v in residuals],
            out_specs=[spec(half)] * 4,
            scratch_shapes=[
                pltpu.VMEM((rows, columns), jnp.float32),
                pltpu.VMEM((len(parts) * part, columns), jnp.bfloat16),
                pltpu.VMEM((1, columns), jnp.float32),
                pltpu.SemaphoreType.DMA((len(parts),)),
            ],
        ),
        compiler_params=pltpu.CompilerParams(vmem_limit_bytes=16 << 20),
        cost_estimate=pl.CostEstimate(
            flops=2 * rows * len(parts) * part * columns,
            bytes_accessed=2 * len(parts) * part * columns,
            transcendentals=0,
        ),
        name="middle",
    )(where, *ins, *parts, *residuals)


def shards(
    conv_value,
    conv_gate,
    conv_weight,
    conv_gain,
    conv_shift,
    out_weight,
    residual,
    mix_gain,
    expert_ids,
    group_weight,
    score_gap,
    w_gate,
    w_up,
    w_down,
):
    row_count, width = conv_value.shape
    taps = conv_weight.shape[0]
    reach = taps - 1
    halo = -(-reach // 16) * 16
    seq_devices = lax.axis_size(("h", "r"))
    half_devices = lax.axis_size("r")
    tp_devices = lax.axis_size("tp")
    far = tp_devices // 2
    quarter = row_count // tp_devices
    capacity = 4 * quarter // seq_devices
    col_count = residual.shape[1]
    tp = lax.axis_index("tp")
    half = lax.axis_index("h")
    share = min(4, half_devices)
    share_at = lax.axis_index("r") % share
    part = width // share

    def mine(value, axis=0):
        return lax.dynamic_slice_in_dim(value, tp * quarter, quarter, axis)

    part_own = swap(lax.dynamic_slice_in_dim(out_weight, share_at * part, part, 0), far)
    parts = [part_own]
    for bit in range(1, share):
        pairs = [(i, i ^ bit) for i in range(half_devices)]
        parts.append(lax.ppermute(part_own, "r", pairs))
    out_blocks = {0: out_weight, far: parts}
    bit = far // 2
    while bit:
        for have in sorted(out_blocks):
            if have < far:
                out_blocks[bit ^ have] = swap(out_blocks[have], bit)
            else:
                pieces = []
                for piece in out_blocks[have]:
                    pieces.append(swap(piece, bit))
                out_blocks[bit ^ have] = pieces
        bit //= 2

    small = jnp.concatenate(
        [conv_weight, conv_gain[None], conv_shift[None], mix_gain.reshape(-1, width)], axis=0
    )
    gated = conv_value.astype(jnp.float32) * jax.nn.sigmoid(conv_gate.astype(jnp.float32))
    gated = gated.astype(jnp.bfloat16)
    previous = lax.ppermute(
        gated[row_count - halo :], ("h", "r"), [(i, i + 1) for i in range(seq_devices - 1)]
    )
    padded = jnp.concatenate([previous, gated], axis=0)
    windows = exchanged(
        lambda bit: lax.dynamic_slice_in_dim(padded, (tp ^ bit) * quarter, halo + quarter, 0),
    )
    smalls = exchanged(lambda bit: small)
    windows[1], w_down = lax.optimization_barrier((windows[1], w_down))
    residuals = exchanged(
        lambda bit: lax.dynamic_slice_in_dim(residual, (tp ^ bit) * quarter, quarter, 0),
    )
    gates = gathered(w_gate[0])
    ups = gathered(w_up[0])
    narrow = col_count // 2

    def columns(value, k):
        return jnp.concatenate(
            [value[:, low : low + narrow] for low in range(k * narrow, D, col_count)], axis=1
        )

    own_downs = [columns(w_down[0], k) for k in (0, 1)]
    downs = [gathered(own_downs[k]) for k in (0, 1)]

    own_about = jnp.concatenate(
        [
            mine(expert_ids.T, 1).astype(jnp.float32),
            mine(group_weight[None], 1),
            mine(score_gap[None], 1),
        ]
    )
    other_about = lax.ppermute(own_about, "h", [(0, 1), (1, 0)])
    order = lax.axis_index("r") if half_devices <= FEW else jnp.int32(0)
    low = half * half_devices
    own_place, *own_gates = routing(own_about, half_devices, capacity, low, order)
    other_place, *other_gates = routing(other_about, half_devices, capacity, low, order)

    act, gains = conv_rows(windows, smalls, taps)
    near = near_product(act, [out_blocks[bit] for bit in range(far)])
    far_blocks = [out_blocks[bit] for bit in range(far, tp_devices)]
    *middle, normed_low, normed_high = middle_rows(
        act, near, gains, far_blocks, residuals, jnp.stack([tp, share_at]).astype(jnp.int32)
    )
    normed = [normed_low, normed_high]

    def inside(blocks):
        if half_devices <= FEW:
            got = [blocks[0]]
            for bit in range(1, half_devices):
                pairs = [(i, i ^ bit) for i in range(half_devices)]
                got.append(lax.ppermute(blocks[bit], "r", pairs))
            return got
        got = lax.all_to_all(
            blocks[0].reshape(half_devices, capacity, -1), "r", 0, 0, tiled=True
        )
        return [got.reshape(half_devices * capacity, -1)]

    def crossed(rows):
        return lax.ppermute(rows, "h", [(0, 1), (1, 0)])

    pieces = half_devices if half_devices <= FEW else 1
    other_parts = [crossed(rows) for rows in normed]
    own_in = inside(placed(own_place, normed, pieces))
    other_in = [inside(placed(other_place, [rows], pieces)) for rows in other_parts]
    places, tops = [], [0, half_devices * capacity]
    for top, parts in zip(tops, ([own_in], other_in)):
        left = 0
        for part in parts:
            places += [(top + i * part[0].shape[0], left) for i in range(len(part))]
            left += part[0].shape[1]
    x_pieces = [block for part in [own_in] + other_in for block in part]
    rows = 2 * half_devices * capacity
    near_own, near_other, x = hidden_rows(x_pieces, places, rows, gates[:far], ups[:far])
    far_own, far_other = hidden_rows([x], [], rows, gates[far:], ups[far:])
    own_hidden, other_hidden = [near_own, far_own], [near_other, far_other]

    outputs = []
    for k in (0, 1):
        across = inside(down_rows(other_hidden, downs[k], pieces))
        back = crossed(weighted(other_gates, across))
        within = inside(down_rows(own_hidden, downs[k], pieces))
        result = weighted(own_gates, within, (middle[k], back))
        rows = natural(
            exchanged(lambda bit: lax.dynamic_slice_in_dim(result, (tp ^ bit) * narrow, narrow, 1)),
            tp,
        )
        outputs.append(jnp.concatenate(rows, axis=0))
    return jnp.concatenate(outputs, axis=1)


def solution(mesh):
    count = mesh.shape["sp"]
    split = Mesh(mesh.devices.reshape(2, count // 2, -1), ("h", "r", "tp"))
    sp = ("h", "r")
    return jax.shard_map(
        shards,
        mesh=split,
        in_specs=(
            P(sp, "tp"),
            P(sp, "tp"),
            P(None, "tp"),
            P("tp"),
            P("tp"),
            P("tp", None),
            P(sp, "tp"),
            P("tp"),
            P(sp, None),
            P(sp),
            P(sp),
            P(sp, None, "tp"),
            P(sp, None, "tp"),
            P(sp, "tp", None),
        ),
        out_specs=P(sp, "tp"),
        check_vma=False,
    )
```

profile of v0, /device:TPU:0, one launch (start us, length us, event | category | flops | bytes accessed | tf_op | source)
XLA Modules:
  0.0 207.6 jit_solution(10944377244299624798)
XLA Ops:
  2.1 2.6 %collective-permute-start.5 = (f32[35,256]{1,0:T(8,128)S(1)}, f32[35,256]{1,0:T(8,128)S(1)}, u32[]{:S(2)}, u32[]{:S(2)}) collective-permute-start(f32[35,256]{1,0:T(8,128)S(1)} %pad_maximum_fusion.2.refs_4_), channel_id=1, source_target_pairs={{0,2},{1,3},{2,0},{3,1},{4,6},{5,7},{6,4},{7,5},{8,10},{9,11},{10,... | collective-permute-start | bytes 107528 | tf_op jit(solution)/shard_map/ppermute | solution.py:20
  5.9 3.4 %collective-permute-start = (bf16[32,256]{1,0:T(8,128)(2,1)S(1)}, bf16[32,256]{1,0:T(8,128)(2,1)S(1)}, u32[]{:S(2)}, u32[]{:S(2)}) collective-permute-start(bf16[32,256]{1,0:T(8,128)(2,1)S(1)} %slice.36), channel_id=1, source_target_pairs={{0,4},{4,8},{8,12},{12,16},{16,20},{20,24},{24,28},{1,5},{5,9},{9,... | collective-permute-start | bytes 49160 | tf_op jit(solution)/shard_map/ppermute | solution.py:506
  12.3 2.7 %collective-permute-start.22 = (f32[4,128]{1,0:T(4,128)S(1)}, f32[4,128]{1,0:T(4,128)S(1)}, u32[]{:S(2)}, u32[]{:S(2)}) collective-permute-start(f32[4,128]{1,0:T(4,128)S(1)} %pad_maximum_fusion.3.refs_1_), channel_id=1, source_target_pairs={{0,16},{16,0},{1,17},{17,1},{2,18},{18,2},{3,19},{19,3},{4,20},{20... | collective-permute-start | bytes 6152 | tf_op jit(solution)/shard_map/ppermute | solution.py:537
  17.1 1.3 collective-permute-start.6
  19.3 1.5 collective-permute-start.9
  20.9 1.6 collective-permute-start.17
  23.3 1.6 collective-permute-start.3
  25.0 5.7 %collective-permute-done.3.refs_3_ = bf16[160,256]{1,0:T(8,128)(2,1)S(1)} collective-permute-done((bf16[160,256]{1,0:T(8,128)(2,1)S(1)}, bf16[160,256]{1,0:T(8,128)(2,1)S(1)}, u32[]{:S(2)}, u32[]{:S(2)}) %collective-permute-start.3) | collective-permute-done | bytes 81952 | tf_op jit(solution)/shard_map/ppermute | solution.py:20
  33.6 1.2 collective-permute-start.10
  35.5 1.3 collective-permute-start.11
  36.8 6.0 %collective-permute-done.10.refs_6_ = bf16[64,2048]{1,0:T(8,128)(2,1)S(1)} collective-permute-done((bf16[64,2048]{1,0:T(8,128)(2,1)S(1)}, bf16[64,2048]{1,0:T(8,128)(2,1)S(1)}, u32[]{:S(2)}, u32[]{:S(2)}) %collective-permute-start.10) | collective-permute-done | bytes 262176 | tf_op jit(solution)/shard_map/ppermute | solution.py:487
  43.5 4.7 %collective-permute-done.11.refs_7_ = bf16[64,2048]{1,0:T(8,128)(2,1)S(1)} collective-permute-done((bf16[64,2048]{1,0:T(8,128)(2,1)S(1)}, bf16[64,2048]{1,0:T(8,128)(2,1)S(1)}, u32[]{:S(2)}, u32[]{:S(2)}) %collective-permute-start.11) | collective-permute-done | bytes 262176 | tf_op jit(solution)/shard_map/ppermute | solution.py:487
  58.4 16.1 %collective-permute-done.33.refs_1_ = bf16[2048,256]{1,0:T(8,128)(2,1)} collective-permute-done((bf16[2048,256]{1,0:T(8,128)(2,1)}, bf16[2048,256]{1,0:T(8,128)(2,1)}, u32[]{:S(2)}, u32[]{:S(2)}) %collective-permute-start.33) | collective-permute-done | bytes 1048608 | tf_op jit(solution)/shard_map/ppermute | solution.py:20
  79.6 2.9 %conv.1 = (bf16[128,1024]{1,0:T(8,128)(2,1)S(1)}, f32[8,256]{1,0:T(8,128)S(1)}) custom-call(bf16[160,256]{1,0:T(8,128)(2,1)S(1)} %get-tuple-element.120.refs_0_, bf16[160,256]{1,0:T(8,128)(2,1)S(1)} %copy-done.36, bf16[160,256]{1,0:T(8,128)(2,1)S(1)} %copy-done.38, bf16[160,256]{1,0:T(8,128)(2,1)S(1)} %copy-done.40, ...), custom_call_target="tpu_custom_call" | custom-call | flops 8126464 | bytes 655360 | tf_op jit(solution)/shard_map/conv/pallas_call | solution.py:315
  82.5 1.2 copy-done.4
  87.8 1.7 middle.1
  90.0 16.4 %collective-permute-done.38.refs_4_ = bf16[256,1024]{1,0:T(8,128)(2,1)S(1)} collective-permute-done((bf16[256,1024]{1,0:T(8,128)(2,1)S(1)}, bf16[256,1024]{1,0:T(8,128)(2,1)S(1)}, u32[]{:S(2)}, u32[]{:S(2)}) %collective-permute-start.38) | collective-permute-done | bytes 524320 | tf_op jit(solution)/shard_map/ppermute | solution.py:20
  107.3 2.4 %collective-permute-start.23 = (bf16[128,1024]{1,0:T(8,128)(2,1)S(1)}, bf16[128,1024]{1,0:T(8,128)(2,1)S(1)}, u32[]{:S(2)}, u32[]{:S(2)}) collective-permute-start(bf16[128,1024]{1,0:T(8,128)(2,1)S(1)} %get-tuple-element.58.refs_1_), channel_id=1, source_target_pairs={{0,16},{16,0},{1,17},{17,1},{2,18},{18,2},{3,19},{19,3},{4,20},{20... | collective-permute-start | bytes 786440 | tf_op jit(solution)/shard_map/ppermute | solution.py:564
  110.6 2.6 %collective-permute-done.19.refs_1_ = bf16[64,2048]{1,0:T(8,128)(2,1)S(1)} collective-permute-done((bf16[64,2048]{1,0:T(8,128)(2,1)S(1)}, bf16[64,2048]{1,0:T(8,128)(2,1)S(1)}, u32[]{:S(2)}, u32[]{:S(2)}) %collective-permute-start.19) | collective-permute-done | bytes 262176 | tf_op jit(solution)/shard_map/ppermute | solution.py:556
  113.2 2.5 %collective-permute-start.21 = (bf16[64,2048]{1,0:T(8,128)(2,1)S(1)}, bf16[64,2048]{1,0:T(8,128)(2,1)S(1)}, u32[]{:S(2)}, u32[]{:S(2)}) collective-permute-start(bf16[64,2048]{1,0:T(8,128)(2,1)S(1)} %get-tuple-element.63), channel_id=1, source_target_pairs={{0,12},{4,8},{8,4},{12,0},{1,13},{5,9},{9,5},{13,1},{2,14},{6,10},... | collective-permute-start | bytes 786440 | tf_op jit(solution)/shard_map/ppermute | solution.py:556
  115.7 7.0 %collective-permute-done.23.refs_1_ = bf16[128,1024]{1,0:T(8,128)(2,1)S(1)} collective-permute-done((bf16[128,1024]{1,0:T(8,128)(2,1)S(1)}, bf16[128,1024]{1,0:T(8,128)(2,1)S(1)}, u32[]{:S(2)}, u32[]{:S(2)}) %collective-permute-start.23) | collective-permute-done | bytes 262176 | tf_op jit(solution)/shard_map/ppermute | solution.py:564
  123.7 1.4 collective-permute-start.24
  125.1 6.9 %collective-permute-done.21.refs_3_ = bf16[64,2048]{1,0:T(8,128)(2,1)S(1)} collective-permute-done((bf16[64,2048]{1,0:T(8,128)(2,1)S(1)}, bf16[64,2048]{1,0:T(8,128)(2,1)S(1)}, u32[]{:S(2)}, u32[]{:S(2)}) %collective-permute-start.21) | collective-permute-done | bytes 262176 | tf_op jit(solution)/shard_map/ppermute | solution.py:556
  132.0 5.1 %collective-permute-done.27.refs_1_ = bf16[128,1024]{1,0:T(8,128)(2,1)S(1)} collective-permute-done((bf16[128,1024]{1,0:T(8,128)(2,1)S(1)}, bf16[128,1024]{1,0:T(8,128)(2,1)S(1)}, u32[]{:S(2)}, u32[]{:S(2)}) %collective-permute-start.27) | collective-permute-done | bytes 262176 | tf_op jit(solution)/shard_map/ppermute | solution.py:564
  138.8 2.1 %collective-permute-start.29 = (bf16[64,1024]{1,0:T(8,128)(2,1)S(1)}, bf16[64,1024]{1,0:T(8,128)(2,1)S(1)}, u32[]{:S(2)}, u32[]{:S(2)}) collective-permute-start(bf16[64,1024]{1,0:T(8,128)(2,1)S(1)} %get-tuple-element.71), channel_id=1, source_target_pairs={{0,8},{4,12},{8,0},{12,4},{1,9},{5,13},{9,1},{13,5},{2,10},{6,14},... | collective-permute-start | bytes 393224 | tf_op jit(solution)/shard_map/ppermute | solution.py:556
  140.9 2.8 %collective-permute-done.26.refs_7_ = bf16[64,1024]{1,0:T(8,128)(2,1)S(1)} collective-permute-done((bf16[64,1024]{1,0:T(8,128)(2,1)S(1)}, bf16[64,1024]{1,0:T(8,128)(2,1)S(1)}, u32[]{:S(2)}, u32[]{:S(2)}) %collective-permute-start.26) | collective-permute-done | bytes 131104 | tf_op jit(solution)/shard_map/ppermute | solution.py:556
  145.8 3.8 %collective-permute-done.30.refs_11_ = bf16[64,1024]{1,0:T(8,128)(2,1)S(1)} collective-permute-done((bf16[64,1024]{1,0:T(8,128)(2,1)S(1)}, bf16[64,1024]{1,0:T(8,128)(2,1)S(1)}, u32[]{:S(2)}, u32[]{:S(2)}) %collective-permute-start.30) | collective-permute-done | bytes 131104 | tf_op jit(solution)/shard_map/ppermute | solution.py:556
  150.1 4.1 %hidden.2 = (bf16[256,512]{1,0:T(8,128)(2,1)S(1)}, bf16[256,512]{1,0:T(8,128)(2,1)S(1)}, bf16[512,2048]{1,0:T(8,128)(2,1)S(1)}) custom-call(bf16[64,2048]{1,0:T(8,128)(2,1)S(1)} %get-tuple-element.60.refs_0_, bf16[64,2048]{1,0:T(8,128)(2,1)S(1)} %collective-permute-done.19.refs_1_, bf16[64,2048]{1,0:T(8,128)(2,1)S(1)} %collective-permute-done.20.refs_2_, ...), custom_call_target="tpu_custom_call" | custom-call | flops 2147483648 | bytes 6815744 | tf_op jit(solution)/shard_map/hidden/pallas_call | solution.py:94
  154.2 4.1 %hidden.3 = (bf16[256,512]{1,0:T(8,128)(2,1)S(1)}, bf16[256,512]{1,0:T(8,128)(2,1)S(1)}) custom-call(bf16[512,2048]{1,0:T(8,128)(2,1)S(1)} %get-tuple-element.74.refs_0_, bf16[2048,256]{1,0:T(8,128)(2,1)} %collective-permute-done.33.refs_1_, bf16[2048,256]{1,0:T(8,128)(2,1)} %collective-permute-done.34.refs_2_, ...), custom_call_target="tpu_custom_call" | custom-call | flops 2147483648 | bytes 6815744 | tf_op jit(solution)/shard_map/hidden/pallas_call | solution.py:94
  159.4 1.5 collective-permute-start.56
  160.9 2.1 collective-permute-start.58
  164.1 1.5 collective-permute-start.43
  165.6 2.1 collective-permute-start.45
  167.7 2.5 %collective-permute-done.58.refs_5_ = bf16[64,1024]{1,0:T(8,128)(2,1)S(1)} collective-permute-done((bf16[64,1024]{1,0:T(8,128)(2,1)S(1)}, bf16[64,1024]{1,0:T(8,128)(2,1)S(1)}, u32[]{:S(2)}, u32[]{:S(2)}) %collective-permute-start.58) | collective-permute-done | bytes 131104 | tf_op jit(solution)/shard_map/ppermute | solution.py:556
  170.2 1.7 weighted.6
  171.9 1.6 collective-permute-start.59
  173.5 1.8 down.6
  176.0 1.9 collective-permute-start.54
  179.9 1.4 collective-permute-start.46
  182.2 1.8 down.4
  184.7 1.4 collective-permute-start.40
  186.2 4.6 %collective-permute-done.55.refs_5_ = bf16[64,1024]{1,0:T(8,128)(2,1)} collective-permute-done((bf16[64,1024]{1,0:T(8,128)(2,1)}, bf16[64,1024]{1,0:T(8,128)(2,1)}, u32[]{:S(2)}, u32[]{:S(2)}) %collective-permute-start.55) | collective-permute-done | bytes 131104 | tf_op jit(solution)/shard_map/ppermute | solution.py:556
  191.7 1.7 weighted.7
  193.6 2.6 %collective-permute-done.41.refs_4_ = bf16[64,1024]{1,0:T(8,128)(2,1)S(1)} collective-permute-done((bf16[64,1024]{1,0:T(8,128)(2,1)}, bf16[64,1024]{1,0:T(8,128)(2,1)S(1)}, u32[]{:S(2)}, u32[]{:S(2)}) %collective-permute-start.41) | collective-permute-done | bytes 131104 | tf_op jit(solution)/shard_map/ppermute | solution.py:556
  196.3 2.2 %collective-permute-done.42.refs_5_ = bf16[64,1024]{1,0:T(8,128)(2,1)S(1)} collective-permute-done((bf16[64,1024]{1,0:T(8,128)(2,1)}, bf16[64,1024]{1,0:T(8,128)(2,1)S(1)}, u32[]{:S(2)}, u32[]{:S(2)}) %collective-permute-start.42) | collective-permute-done | bytes 131104 | tf_op jit(solution)/shard_map/ppermute | solution.py:556
  199.4 2.0 weighted.5
  201.5 1.2 collective-permute-start.48
  203.5 2.4 %collective-permute-done.47 = bf16[128,256]{1,0:T(8,128)(2,1)S(1)} collective-permute-done((bf16[128,256]{1,0:T(8,128)(2,1)S(1)}, bf16[128,256]{1,0:T(8,128)(2,1)S(1)}, u32[]{:S(2)}, u32[]{:S(2)}) %collective-permute-start.47) | collective-permute-done | bytes 65568 | tf_op jit(solution)/shard_map/ppermute | solution.py:20
  (214 shorter events, 52.7 us)
Async XLA Ops:
  1.6 17.2 %collective-permute-start.4 = (f32[35,256]{1,0:T(8,128)S(1)}, f32[35,256]{1,0:T(8,128)S(1)}, u32[]{:S(2)}, u32[]{:S(2)}) collective-permute-start(f32[35,256]{1,0:T(8,128)S(1)} %pad_maximum_fusion.2.refs_4_), channel_id=1, source_target_pairs={{0,1},{1,0},{2,3},{3,2},{4,5},{5,4},{6,7},{7,6},{8,9},{9,8},{10,11... | collective-permute-start | bytes 107528 | tf_op jit(solution)/shard_map/ppermute | solution.py:20
  2.1 18.8 %collective-permute-start.5 = (f32[35,256]{1,0:T(8,128)S(1)}, f32[35,256]{1,0:T(8,128)S(1)}, u32[]{:S(2)}, u32[]{:S(2)}) collective-permute-start(f32[35,256]{1,0:T(8,128)S(1)} %pad_maximum_fusion.2.refs_4_), channel_id=1, source_target_pairs={{0,2},{1,3},{2,0},{3,1},{4,6},{5,7},{6,4},{7,5},{8,10},{9,11},{10,... | collective-permute-start | bytes 107528 | tf_op jit(solution)/shard_map/ppermute | solution.py:20
  5.9 9.1 %collective-permute-start = (bf16[32,256]{1,0:T(8,128)(2,1)S(1)}, bf16[32,256]{1,0:T(8,128)(2,1)S(1)}, u32[]{:S(2)}, u32[]{:S(2)}) collective-permute-start(bf16[32,256]{1,0:T(8,128)(2,1)S(1)} %slice.36), channel_id=1, source_target_pairs={{0,4},{4,8},{8,12},{12,16},{16,20},{20,24},{24,28},{1,5},{5,9},{9,... | collective-permute-start | bytes 49160 | tf_op jit(solution)/shard_map/ppermute | solution.py:506
  10.3 9.0 %collective-permute-start.8 = (bf16[64,2048]{1,0:T(8,128)(2,1)S(1)}, bf16[64,2048]{1,0:T(8,128)(2,1)S(1)}, u32[]{:S(2)}, u32[]{:S(2)}) collective-permute-start(bf16[64,2048]{1,0:T(8,128)(2,1)S(1)} %constant_dynamic-slice_fusion.10), channel_id=1, source_target_pairs={{0,2},{1,3},{2,0},{3,1},{4,6},{5,7},{6,4},{7,5},{8,10},{9,11},{10,... | collective-permute-start | bytes 786440 | tf_op jit(solution)/shard_map/ppermute | solution.py:20
  18.4 13.4 %collective-permute-start.16 = (bf16[128,512]{1,0:T(8,128)(2,1)S(1)}, bf16[128,512]{1,0:T(8,128)(2,1)S(1)}, u32[]{:S(2)}, u32[]{:S(2)}) collective-permute-start(bf16[128,512]{1,0:T(8,128)(2,1)S(1)} %get-tuple-element.108), channel_id=1, source_target_pairs={{0,1},{1,0},{2,3},{3,2},{4,5},{5,4},{6,7},{7,6},{8,9},{9,8},{10,11... | collective-permute-start | bytes 393224 | tf_op jit(solution)/shard_map/ppermute | solution.py:20
  19.3 17.5 %collective-permute-start.9 = (bf16[64,2048]{1,0:T(8,128)(2,1)S(1)}, bf16[64,2048]{1,0:T(8,128)(2,1)S(1)}, u32[]{:S(2)}, u32[]{:S(2)}) collective-permute-start(bf16[64,2048]{1,0:T(8,128)(2,1)S(1)} %collective-permute-done.8.refs_4_), channel_id=1, source_target_pairs={{0,4},{4,0},{8,12},{12,8},{1,5},{5,1},{9,13},{13,9},{2,6},{6,2},{1... | collective-permute-start | bytes 786440 | tf_op jit(solution)/shard_map/ppermute | solution.py:487
  20.9 12.0 %collective-permute-start.17 = (bf16[128,512]{1,0:T(8,128)(2,1)S(1)}, bf16[128,512]{1,0:T(8,128)(2,1)S(1)}, u32[]{:S(2)}, u32[]{:S(2)}) collective-permute-start(bf16[128,512]{1,0:T(8,128)(2,1)S(1)} %get-tuple-element.110), channel_id=1, source_target_pairs={{0,2},{1,3},{2,0},{3,1},{4,6},{5,7},{6,4},{7,5},{8,10},{9,11},{10,... | collective-permute-start | bytes 393224 | tf_op jit(solution)/shard_map/ppermute | solution.py:20
  23.1 11.7 %collective-permute-start.18 = (bf16[128,512]{1,0:T(8,128)(2,1)S(1)}, bf16[128,512]{1,0:T(8,128)(2,1)S(1)}, u32[]{:S(2)}, u32[]{:S(2)}) collective-permute-start(bf16[128,512]{1,0:T(8,128)(2,1)S(1)} %get-tuple-element.107), channel_id=1, source_target_pairs={{0,3},{1,2},{2,1},{3,0},{4,7},{5,6},{6,5},{7,4},{8,11},{9,10},{10,... | collective-permute-start | bytes 393224 | tf_op jit(solution)/shard_map/ppermute | solution.py:20
  23.3 7.3 %collective-permute-start.3 = (bf16[160,256]{1,0:T(8,128)(2,1)S(1)}, bf16[160,256]{1,0:T(8,128)(2,1)S(1)}, u32[]{:S(2)}, u32[]{:S(2)}) collective-permute-start(bf16[160,256]{1,0:T(8,128)(2,1)S(1)} %get-tuple-element.119), channel_id=1, source_target_pairs={{0,3},{1,2},{2,1},{3,0},{4,7},{5,6},{6,5},{7,4},{8,11},{9,10},{10,... | collective-permute-start | bytes 245768 | tf_op jit(solution)/shard_map/ppermute | solution.py:20
  31.3 19.3 %collective-permute-start.51 = (bf16[256,1024]{1,0:T(8,128)(2,1)S(1)}, bf16[256,1024]{1,0:T(8,128)(2,1)S(1)}, u32[]{:S(2)}, u32[]{:S(2)}) collective-permute-start(bf16[256,1024]{1,0:T(8,128)(2,1)S(1)} %pad_maximum_fusion.1.refs_2_), channel_id=1, source_target_pairs={{0,2},{1,3},{2,0},{3,1},{4,6},{5,7},{6,4},{7,5},{8,10},{9,11},{10,... | collective-permute-start | bytes 1572872 | tf_op jit(solution)/shard_map/ppermute | solution.py:20
  32.5 23.1 %collective-permute-start.7 = (bf16[256,2048]{1,0:T(8,128)(2,1)S(1)}, bf16[256,2048]{1,0:T(8,128)(2,1)S(1)}, u32[]{:S(2)}, u32[]{:S(2)}) collective-permute-start(bf16[256,2048]{1,0:T(8,128)(2,1)S(1)} %copy-done), channel_id=1, source_target_pairs={{0,1},{1,0},{2,3},{3,2},{4,5},{5,4},{6,7},{7,6},{8,9},{9,8},{10,11... | collective-permute-start | bytes 3145736 | tf_op jit(solution)/shard_map/ppermute | solution.py:20
  33.6 9.2 %collective-permute-start.10 = (bf16[64,2048]{1,0:T(8,128)(2,1)S(1)}, bf16[64,2048]{1,0:T(8,128)(2,1)S(1)}, u32[]{:S(2)}, u32[]{:S(2)}) collective-permute-start(bf16[64,2048]{1,0:T(8,128)(2,1)S(1)} %collective-permute-done.8.refs_4_), channel_id=1, source_target_pairs={{0,8},{4,12},{8,0},{12,4},{1,9},{5,13},{9,1},{13,5},{2,10},{6,14},... | collective-permute-start | bytes 786440 | tf_op jit(solution)/shard_map/ppermute | solution.py:487
  35.5 12.7 %collective-permute-start.11 = (bf16[64,2048]{1,0:T(8,128)(2,1)S(1)}, bf16[64,2048]{1,0:T(8,128)(2,1)S(1)}, u32[]{:S(2)}, u32[]{:S(2)}) collective-permute-start(bf16[64,2048]{1,0:T(8,128)(2,1)S(1)} %collective-permute-done.8.refs_4_), channel_id=1, source_target_pairs={{0,12},{4,8},{8,4},{12,0},{1,13},{5,9},{9,5},{13,1},{2,14},{6,10},... | collective-permute-start | bytes 786440 | tf_op jit(solution)/shard_map/ppermute | solution.py:487
  36.8 12.3 %collective-permute-start.12 = (bf16[64,2048]{1,0:T(8,128)(2,1)S(1)}, bf16[64,2048]{1,0:T(8,128)(2,1)S(1)}, u32[]{:S(2)}, u32[]{:S(2)}) collective-permute-start(bf16[64,2048]{1,0:T(8,128)(2,1)S(1)} %collective-permute-done.8.refs_4_), channel_id=1, source_target_pairs={{0,1},{1,0},{2,3},{3,2},{4,5},{5,4},{6,7},{7,6},{8,9},{9,8},{10,11... | collective-permute-start | bytes 786440 | tf_op jit(solution)/shard_map/ppermute | solution.py:20
  42.8 9.1 %collective-permute-start.13 = (bf16[64,2048]{1,0:T(8,128)(2,1)S(1)}, bf16[64,2048]{1,0:T(8,128)(2,1)S(1)}, u32[]{:S(2)}, u32[]{:S(2)}) collective-permute-start(bf16[64,2048]{1,0:T(8,128)(2,1)S(1)} %collective-permute-done.9.refs_5_), channel_id=1, source_target_pairs={{0,1},{1,0},{2,3},{3,2},{4,5},{5,4},{6,7},{7,6},{8,9},{9,8},{10,11... | collective-permute-start | bytes 786440 | tf_op jit(solution)/shard_map/ppermute | solution.py:20
  48.1 26.3 %collective-permute-start.33 = (bf16[2048,256]{1,0:T(8,128)(2,1)}, bf16[2048,256]{1,0:T(8,128)(2,1)}, u32[]{:S(2)}, u32[]{:S(2)}) collective-permute-start(bf16[2048,256]{1,0:T(8,128)(2,1)} %bitcast.9.refs_12_), channel_id=1, source_target_pairs={{0,2},{1,3},{2,0},{3,1},{4,6},{5,7},{6,4},{7,5},{8,10},{9,11},{10,... | collective-permute-start | bytes 3145736 | tf_op jit(solution)/shard_map/ppermute | solution.py:20
  52.5 54.8 %collective-permute-start.34 = (bf16[2048,256]{1,0:T(8,128)(2,1)}, bf16[2048,256]{1,0:T(8,128)(2,1)}, u32[]{:S(2)}, u32[]{:S(2)}) collective-permute-start(bf16[2048,256]{1,0:T(8,128)(2,1)} %bitcast.10.refs_13_), channel_id=1, source_target_pairs={{0,2},{1,3},{2,0},{3,1},{4,6},{5,7},{6,4},{7,5},{8,10},{9,11},{10,... | collective-permute-start | bytes 3145736 | tf_op jit(solution)/shard_map/ppermute | solution.py:20
  54.3 53.0 %collective-permute-start.31 = (bf16[2048,256]{1,0:T(8,128)(2,1)}, bf16[2048,256]{1,0:T(8,128)(2,1)}, u32[]{:S(2)}, u32[]{:S(2)}) collective-permute-start(bf16[2048,256]{1,0:T(8,128)(2,1)} %bitcast.9.refs_12_), channel_id=1, source_target_pairs={{0,1},{1,0},{2,3},{3,2},{4,5},{5,4},{6,7},{7,6},{8,9},{9,8},{10,11... | collective-permute-start | bytes 3145736 | tf_op jit(solution)/shard_map/ppermute | solution.py:20
  55.0 54.7 %collective-permute-start.32 = (bf16[2048,256]{1,0:T(8,128)(2,1)}, bf16[2048,256]{1,0:T(8,128)(2,1)}, u32[]{:S(2)}, u32[]{:S(2)}) collective-permute-start(bf16[2048,256]{1,0:T(8,128)(2,1)} %bitcast.10.refs_13_), channel_id=1, source_target_pairs={{0,1},{1,0},{2,3},{3,2},{4,5},{5,4},{6,7},{7,6},{8,9},{9,8},{10,11... | collective-permute-start | bytes 3145736 | tf_op jit(solution)/shard_map/ppermute | solution.py:20
  56.6 49.9 %collective-permute-start.38 = (bf16[256,1024]{1,0:T(8,128)(2,1)S(1)}, bf16[256,1024]{1,0:T(8,128)(2,1)S(1)}, u32[]{:S(2)}, u32[]{:S(2)}) collective-permute-start(bf16[256,1024]{1,0:T(8,128)(2,1)S(1)} %pad_maximum_fusion.refs_2_), channel_id=1, source_target_pairs={{0,2},{1,3},{2,0},{3,1},{4,6},{5,7},{6,4},{7,5},{8,10},{9,11},{10,... | collective-permute-start | bytes 1572872 | tf_op jit(solution)/shard_map/ppermute | solution.py:20
  74.5 75.1 %collective-permute-start.35 = (bf16[2048,256]{1,0:T(8,128)(2,1)}, bf16[2048,256]{1,0:T(8,128)(2,1)S(1)}, u32[]{:S(2)}, u32[]{:S(2)}) collective-permute-start(bf16[2048,256]{1,0:T(8,128)(2,1)} %collective-permute-done.33.refs_1_), channel_id=1, source_target_pairs={{0,1},{1,0},{2,3},{3,2},{4,5},{5,4},{6,7},{7,6},{8,9},{9,8},{10,11... | collective-permute-start | bytes 3145736 | tf_op jit(solution)/shard_map/ppermute | solution.py:20
  107.3 46.9 %collective-permute-start.36 = (bf16[2048,256]{1,0:T(8,128)(2,1)}, bf16[2048,256]{1,0:T(8,128)(2,1)S(1)}, u32[]{:S(2)}, u32[]{:S(2)}) collective-permute-start(bf16[2048,256]{1,0:T(8,128)(2,1)} %collective-permute-done.34.refs_2_), channel_id=1, source_target_pairs={{0,1},{1,0},{2,3},{3,2},{4,5},{5,4},{6,7},{7,6},{8,9},{9,8},{10,11... | collective-permute-start | bytes 3145736 | tf_op jit(solution)/shard_map/ppermute | solution.py:20
  107.3 15.3 %collective-permute-start.23 = (bf16[128,1024]{1,0:T(8,128)(2,1)S(1)}, bf16[128,1024]{1,0:T(8,128)(2,1)S(1)}, u32[]{:S(2)}, u32[]{:S(2)}) collective-permute-start(bf16[128,1024]{1,0:T(8,128)(2,1)S(1)} %get-tuple-element.58.refs_1_), channel_id=1, source_target_pairs={{0,16},{16,0},{1,17},{17,1},{2,18},{18,2},{3,19},{19,3},{4,20},{20... | collective-permute-start | bytes 786440 | tf_op jit(solution)/shard_map/ppermute | solution.py:564
  109.7 14.0 %collective-permute-start.20 = (bf16[64,2048]{1,0:T(8,128)(2,1)S(1)}, bf16[64,2048]{1,0:T(8,128)(2,1)S(1)}, u32[]{:S(2)}, u32[]{:S(2)}) collective-permute-start(bf16[64,2048]{1,0:T(8,128)(2,1)S(1)} %get-tuple-element.62), channel_id=1, source_target_pairs={{0,8},{4,12},{8,0},{12,4},{1,9},{5,13},{9,1},{13,5},{2,10},{6,14},... | collective-permute-start | bytes 786440 | tf_op jit(solution)/shard_map/ppermute | solution.py:556
  113.2 18.8 %collective-permute-start.21 = (bf16[64,2048]{1,0:T(8,128)(2,1)S(1)}, bf16[64,2048]{1,0:T(8,128)(2,1)S(1)}, u32[]{:S(2)}, u32[]{:S(2)}) collective-permute-start(bf16[64,2048]{1,0:T(8,128)(2,1)S(1)} %get-tuple-element.63), channel_id=1, source_target_pairs={{0,12},{4,8},{8,4},{12,0},{1,13},{5,9},{9,5},{13,1},{2,14},{6,10},... | collective-permute-start | bytes 786440 | tf_op jit(solution)/shard_map/ppermute | solution.py:556
  122.7 14.4 %collective-permute-start.27 = (bf16[128,1024]{1,0:T(8,128)(2,1)S(1)}, bf16[128,1024]{1,0:T(8,128)(2,1)S(1)}, u32[]{:S(2)}, u32[]{:S(2)}) collective-permute-start(bf16[128,1024]{1,0:T(8,128)(2,1)S(1)} %get-tuple-element.59.refs_2_), channel_id=1, source_target_pairs={{0,16},{16,0},{1,17},{17,1},{2,18},{18,2},{3,19},{19,3},{4,20},{20... | collective-permute-start | bytes 786440 | tf_op jit(solution)/shard_map/ppermute | solution.py:564
  123.7 13.9 %collective-permute-start.24 = (bf16[64,1024]{1,0:T(8,128)(2,1)S(1)}, bf16[64,1024]{1,0:T(8,128)(2,1)S(1)}, u32[]{:S(2)}, u32[]{:S(2)}) collective-permute-start(bf16[64,1024]{1,0:T(8,128)(2,1)S(1)} %get-tuple-element.66), channel_id=1, source_target_pairs={{0,4},{4,0},{8,12},{12,8},{1,5},{5,1},{9,13},{13,9},{2,6},{6,2},{1... | collective-permute-start | bytes 393224 | tf_op jit(solution)/shard_map/ppermute | solution.py:556
  137.7 7.1 %collective-permute-start.28 = (bf16[64,1024]{1,0:T(8,128)(2,1)S(1)}, bf16[64,1024]{1,0:T(8,128)(2,1)S(1)}, u32[]{:S(2)}, u32[]{:S(2)}) collective-permute-start(bf16[64,1024]{1,0:T(8,128)(2,1)S(1)} %get-tuple-element.70), channel_id=1, source_target_pairs={{0,4},{4,0},{8,12},{12,8},{1,5},{5,1},{9,13},{13,9},{2,6},{6,2},{1... | collective-permute-start | bytes 393224 | tf_op jit(solution)/shard_map/ppermute | solution.py:556
  138.8 7.0 %collective-permute-start.29 = (bf16[64,1024]{1,0:T(8,128)(2,1)S(1)}, bf16[64,1024]{1,0:T(8,128)(2,1)S(1)}, u32[]{:S(2)}, u32[]{:S(2)}) collective-permute-start(bf16[64,1024]{1,0:T(8,128)(2,1)S(1)} %get-tuple-element.71), channel_id=1, source_target_pairs={{0,8},{4,12},{8,0},{12,4},{1,9},{5,13},{9,1},{13,5},{2,10},{6,14},... | collective-permute-start | bytes 393224 | tf_op jit(solution)/shard_map/ppermute | solution.py:556
  144.8 13.5 %collective-permute-start.50 = (bf16[256,1024]{1,0:T(8,128)(2,1)S(1)}, bf16[256,1024]{1,0:T(8,128)(2,1)S(1)}, u32[]{:S(2)}, u32[]{:S(2)}) collective-permute-start(bf16[256,1024]{1,0:T(8,128)(2,1)S(1)} %pad_maximum_fusion.1.refs_2_), channel_id=1, source_target_pairs={{0,1},{1,0},{2,3},{3,2},{4,5},{5,4},{6,7},{7,6},{8,9},{9,8},{10,11... | collective-permute-start | bytes 1572872 | tf_op jit(solution)/shard_map/ppermute | solution.py:20
  145.8 12.5 %collective-permute-start.52 = (bf16[256,1024]{1,0:T(8,128)(2,1)S(1)}, bf16[256,1024]{1,0:T(8,128)(2,1)S(1)}, u32[]{:S(2)}, u32[]{:S(2)}) collective-permute-start(bf16[256,1024]{1,0:T(8,128)(2,1)S(1)} %collective-permute-done.51.refs_4_), channel_id=1, source_target_pairs={{0,1},{1,0},{2,3},{3,2},{4,5},{5,4},{6,7},{7,6},{8,9},{9,8},{10,11... | collective-permute-start | bytes 1572872 | tf_op jit(solution)/shard_map/ppermute | solution.py:20
  149.6 13.4 %collective-permute-start.37 = (bf16[256,1024]{1,0:T(8,128)(2,1)S(1)}, bf16[256,1024]{1,0:T(8,128)(2,1)S(1)}, u32[]{:S(2)}, u32[]{:S(2)}) collective-permute-start(bf16[256,1024]{1,0:T(8,128)(2,1)S(1)} %pad_maximum_fusion.refs_2_), channel_id=1, source_target_pairs={{0,1},{1,0},{2,3},{3,2},{4,5},{5,4},{6,7},{7,6},{8,9},{9,8},{10,11... | collective-permute-start | bytes 1572872 | tf_op jit(solution)/shard_map/ppermute | solution.py:20
  149.6 13.4 %collective-permute-start.39 = (bf16[256,1024]{1,0:T(8,128)(2,1)S(1)}, bf16[256,1024]{1,0:T(8,128)(2,1)S(1)}, u32[]{:S(2)}, u32[]{:S(2)}) collective-permute-start(bf16[256,1024]{1,0:T(8,128)(2,1)S(1)} %collective-permute-done.38.refs_4_), channel_id=1, source_target_pairs={{0,1},{1,0},{2,3},{3,2},{4,5},{5,4},{6,7},{7,6},{8,9},{9,8},{10,11... | collective-permute-start | bytes 1572872 | tf_op jit(solution)/shard_map/ppermute | solution.py:20
  160.9 9.2 %collective-permute-start.58 = (bf16[64,1024]{1,0:T(8,128)(2,1)S(1)}, bf16[64,1024]{1,0:T(8,128)(2,1)S(1)}, u32[]{:S(2)}, u32[]{:S(2)}) collective-permute-start(bf16[64,1024]{1,0:T(8,128)(2,1)S(1)} %get-tuple-element.98), channel_id=1, source_target_pairs={{0,12},{4,8},{8,4},{12,0},{1,13},{5,9},{9,5},{13,1},{2,14},{6,10},... | collective-permute-start | bytes 393224 | tf_op jit(solution)/shard_map/ppermute | solution.py:556
  164.1 11.9 %collective-permute-start.43 = (bf16[64,1024]{1,0:T(8,128)(2,1)S(1)}, bf16[64,1024]{1,0:T(8,128)(2,1)S(1)}, u32[]{:S(2)}, u32[]{:S(2)}) collective-permute-start(bf16[64,1024]{1,0:T(8,128)(2,1)S(1)} %get-tuple-element.87), channel_id=1, source_target_pairs={{0,4},{4,0},{8,12},{12,8},{1,5},{5,1},{9,13},{13,9},{2,6},{6,2},{1... | collective-permute-start | bytes 393224 | tf_op jit(solution)/shard_map/ppermute | solution.py:556
  165.6 12.3 %collective-permute-start.44 = (bf16[64,1024]{1,0:T(8,128)(2,1)S(1)}, bf16[64,1024]{1,0:T(8,128)(2,1)S(1)}, u32[]{:S(2)}, u32[]{:S(2)}) collective-permute-start(bf16[64,1024]{1,0:T(8,128)(2,1)S(1)} %get-tuple-element.88), channel_id=1, source_target_pairs={{0,8},{4,12},{8,0},{12,4},{1,9},{5,13},{9,1},{13,5},{2,10},{6,14},... | collective-permute-start | bytes 393224 | tf_op jit(solution)/shard_map/ppermute | solution.py:556
  165.6 13.2 %collective-permute-start.45 = (bf16[64,1024]{1,0:T(8,128)(2,1)S(1)}, bf16[64,1024]{1,0:T(8,128)(2,1)S(1)}, u32[]{:S(2)}, u32[]{:S(2)}) collective-permute-start(bf16[64,1024]{1,0:T(8,128)(2,1)S(1)} %get-tuple-element.89), channel_id=1, source_target_pairs={{0,12},{4,8},{8,4},{12,0},{1,13},{5,9},{9,5},{13,1},{2,14},{6,10},... | collective-permute-start | bytes 393224 | tf_op jit(solution)/shard_map/ppermute | solution.py:556
  171.9 19.0 %collective-permute-start.59 = (bf16[128,1024]{1,0:T(8,128)(2,1)}, bf16[128,1024]{1,0:T(8,128)(2,1)}, u32[]{:S(2)}, u32[]{:S(2)}) collective-permute-start(bf16[128,1024]{1,0:T(8,128)(2,1)} %weighted.6), channel_id=1, source_target_pairs={{0,16},{16,0},{1,17},{17,1},{2,18},{18,2},{3,19},{19,3},{4,20},{20... | collective-permute-start | bytes 786440 | tf_op jit(solution)/shard_map/ppermute | solution.py:564
  175.3 9.4 %collective-permute-start.53 = (bf16[64,1024]{1,0:T(8,128)(2,1)}, bf16[64,1024]{1,0:T(8,128)(2,1)}, u32[]{:S(2)}, u32[]{:S(2)}) collective-permute-start(bf16[64,1024]{1,0:T(8,128)(2,1)} %get-tuple-element.91), channel_id=1, source_target_pairs={{0,4},{4,0},{8,12},{12,8},{1,5},{5,1},{9,13},{13,9},{2,6},{6,2},{1... | collective-permute-start | bytes 393224 | tf_op jit(solution)/shard_map/ppermute | solution.py:556
  176.0 10.2 %collective-permute-start.54 = (bf16[64,1024]{1,0:T(8,128)(2,1)}, bf16[64,1024]{1,0:T(8,128)(2,1)}, u32[]{:S(2)}, u32[]{:S(2)}) collective-permute-start(bf16[64,1024]{1,0:T(8,128)(2,1)} %get-tuple-element.92), channel_id=1, source_target_pairs={{0,8},{4,12},{8,0},{12,4},{1,9},{5,13},{9,1},{13,5},{2,10},{6,14},... | collective-permute-start | bytes 393224 | tf_op jit(solution)/shard_map/ppermute | solution.py:556
  178.0 12.9 %collective-permute-start.55 = (bf16[64,1024]{1,0:T(8,128)(2,1)}, bf16[64,1024]{1,0:T(8,128)(2,1)}, u32[]{:S(2)}, u32[]{:S(2)}) collective-permute-start(bf16[64,1024]{1,0:T(8,128)(2,1)} %get-tuple-element.93), channel_id=1, source_target_pairs={{0,12},{4,8},{8,4},{12,0},{1,13},{5,9},{9,5},{13,1},{2,14},{6,10},... | collective-permute-start | bytes 393224 | tf_op jit(solution)/shard_map/ppermute | solution.py:556
  179.9 18.6 %collective-permute-start.46 = (bf16[128,1024]{1,0:T(8,128)(2,1)S(1)}, bf16[128,1024]{1,0:T(8,128)(2,1)}, u32[]{:S(2)}, u32[]{:S(2)}) collective-permute-start(bf16[128,1024]{1,0:T(8,128)(2,1)S(1)} %weighted.4), channel_id=1, source_target_pairs={{0,16},{16,0},{1,17},{17,1},{2,18},{18,2},{3,19},{19,3},{4,20},{20... | collective-permute-start | bytes 786440 | tf_op jit(solution)/shard_map/ppermute | solution.py:564
  184.7 8.9 %collective-permute-start.40 = (bf16[64,1024]{1,0:T(8,128)(2,1)}, bf16[64,1024]{1,0:T(8,128)(2,1)S(1)}, u32[]{:S(2)}, u32[]{:S(2)}) collective-permute-start(bf16[64,1024]{1,0:T(8,128)(2,1)} %get-tuple-element.78), channel_id=1, source_target_pairs={{0,4},{4,0},{8,12},{12,8},{1,5},{5,1},{9,13},{13,9},{2,6},{6,2},{1... | collective-permute-start | bytes 393224 | tf_op jit(solution)/shard_map/ppermute | solution.py:556
  186.2 10.1 %collective-permute-start.41 = (bf16[64,1024]{1,0:T(8,128)(2,1)}, bf16[64,1024]{1,0:T(8,128)(2,1)S(1)}, u32[]{:S(2)}, u32[]{:S(2)}) collective-permute-start(bf16[64,1024]{1,0:T(8,128)(2,1)} %get-tuple-element.79), channel_id=1, source_target_pairs={{0,8},{4,12},{8,0},{12,4},{1,9},{5,13},{9,1},{13,5},{2,10},{6,14},... | collective-permute-start | bytes 393224 | tf_op jit(solution)/shard_map/ppermute | solution.py:556
  190.8 7.6 %collective-permute-start.42 = (bf16[64,1024]{1,0:T(8,128)(2,1)}, bf16[64,1024]{1,0:T(8,128)(2,1)S(1)}, u32[]{:S(2)}, u32[]{:S(2)}) collective-permute-start(bf16[64,1024]{1,0:T(8,128)(2,1)} %get-tuple-element.80), channel_id=1, source_target_pairs={{0,12},{4,8},{8,4},{12,0},{1,13},{5,9},{9,5},{13,1},{2,14},{6,10},... | collective-permute-start | bytes 393224 | tf_op jit(solution)/shard_map/ppermute | solution.py:556
  193.5 9.3 %collective-permute-start.60 = (bf16[128,256]{1,0:T(8,128)(2,1)S(1)}, bf16[128,256]{1,0:T(8,128)(2,1)S(1)}, u32[]{:S(2)}, u32[]{:S(2)}) collective-permute-start(bf16[128,256]{1,0:T(8,128)(2,1)S(1)} %get-tuple-element.128), channel_id=1, source_target_pairs={{0,3},{1,2},{2,1},{3,0},{4,7},{5,6},{6,5},{7,4},{8,11},{9,10},{10,... | collective-permute-start | bytes 196616 | tf_op jit(solution)/shard_map/ppermute | solution.py:20
  193.6 9.8 %collective-permute-start.61 = (bf16[128,256]{1,0:T(8,128)(2,1)S(1)}, bf16[128,256]{1,0:T(8,128)(2,1)S(1)}, u32[]{:S(2)}, u32[]{:S(2)}) collective-permute-start(bf16[128,256]{1,0:T(8,128)(2,1)S(1)} %get-tuple-element.127), channel_id=1, source_target_pairs={{0,2},{1,3},{2,0},{3,1},{4,6},{5,7},{6,4},{7,5},{8,10},{9,11},{10,... | collective-permute-start | bytes 196616 | tf_op jit(solution)/shard_map/ppermute | solution.py:20
  196.3 7.1 %collective-permute-start.62 = (bf16[128,256]{1,0:T(8,128)(2,1)S(1)}, bf16[128,256]{1,0:T(8,128)(2,1)S(1)}, u32[]{:S(2)}, u32[]{:S(2)}) collective-permute-start(bf16[128,256]{1,0:T(8,128)(2,1)S(1)} %get-tuple-element.126), channel_id=1, source_target_pairs={{0,1},{1,0},{2,3},{3,2},{4,5},{5,4},{6,7},{7,6},{8,9},{9,8},{10,11... | collective-permute-start | bytes 196616 | tf_op jit(solution)/shard_map/ppermute | solution.py:20
  (64 other events, 410.3 us)
where the time goes:
time: 208 us
  waiting for transfers between devices  95.3 us (46%)
  starting transfers between devices  53.9 us (26%)
  Pallas kernels  28.6 us (14%)
  local copies, waits for them, and re-layouts  25.2 us (12%)
  other arithmetic  4.06 us (2%)
    ppermute x33, waiting for transfers between devices, swap(): lax.ppermute(value, 'tp', [(source, source ^ bit) for source in range(cou...  42.9 us
    ppermute x21, waiting for transfers between devices, inside(): got.append(lax.ppermute(blocks[bit], 'r', pairs))  29.7 us
    unnamed x98, local copies, waits for them, and re-layouts  22.5 us
    ppermute x21, starting transfers between devices, inside(): got.append(lax.ppermute(blocks[bit], 'r', pairs))  21.7 us
    ppermute x33, starting transfers between devices, swap(): lax.ppermute(value, 'tp', [(source, source ^ bit) for source in range(cou...  16.7 us
    ppermute x4, waiting for transfers between devices, crossed(): return lax.ppermute(rows, 'h', [(0, 1), (1, 0)])  12 us
    ppermute x3, waiting for transfers between devices, shards(): parts.append(lax.ppermute(part_own, 'r', pairs))  10.6 us
    pallas_call x2, Pallas kernels, hidden_rows(): pl.pallas_call(lambda *refs: hidden_kernel(places, blocks, *refs), out_sh...  8.19 us
  transfers between devices with their start and end apart: 63, of which 21 were waited for; matrix products, arithmetic and copies ran while one was open for 2% of the time, Pallas kernels for 14%

commit v1 on v0

--- a/solution.py
+++ b/solution.py
@@ -108,7 +108,7 @@
             bytes_accessed=2 * (rows * depth + blocks * width * (2 * depth + rows)),
             transcendentals=blocks * rows * width,
         ),
-        name="hidden",
+        name="hid",
     )(*pieces, *weights)
 
 
@@ -353,14 +353,14 @@
         out_shape=jax.ShapeDtypeStruct((rows, columns), jnp.float32),
         grid=(columns // tile,),
         in_specs=[whole(act.shape)] + [pl.BlockSpec((width, tile), lambda i: (0, i))] * len(weights),
-        out_specs=pl.BlockSpec((rows, tile), lambda i: (0, i)),
+        out_specs=pl.BlockSpec((rows, tile), lambda i: (0, i), memory_space=pltpu.VMEM),
         compiler_params=pltpu.CompilerParams(vmem_limit_bytes=16 << 20),
         cost_estimate=pl.CostEstimate(
             flops=2 * rows * width * columns * len(weights),
             bytes_accessed=2 * width * columns * len(weights),
             transcendentals=0,
         ),
-        name="near_product",
+        name="near",
     )(act, *weights)
 
 
@@ -423,7 +423,7 @@
         grid_spec=pltpu.PrefetchScalarGridSpec(
             num_scalar_prefetch=1,
             grid=(1,),
-            in_specs=[spec(v.shape) for v in ins]
+            in_specs=[pl.BlockSpec(memory_space=pltpu.VMEM)] * len(ins)
             + [pl.BlockSpec(memory_space=pl.ANY)] * len(parts)
             + [spec(v.shape) for v in residuals],
             out_specs=[spec(half)] * 4,

time: 208 us -> 208 us (level)
  no operation moved by 1% of the time
where the time goes in v1:
time: 208 us
  waiting for transfers between devices  95.3 us (46%)
  starting transfers between devices  53.9 us (26%)
  Pallas kernels  28.6 us (14%)
  local copies, waits for them, and re-layouts  25.2 us (12%)
  other arithmetic  4.06 us (2%)
    ppermute x33, waiting for transfers between devices, swap(): lax.ppermute(value, 'tp', [(source, source ^ bit) for source in range(cou...  42.9 us
    ppermute x21, waiting for transfers between devices, inside(): got.append(lax.ppermute(blocks[bit], 'r', pairs))  29.7 us
    unnamed x98, local copies, waits for them, and re-layouts  22.5 us
    ppermute x21, starting transfers between devices, inside(): got.append(lax.ppermute(blocks[bit], 'r', pairs))  21.7 us
    ppermute x33, starting transfers between devices, swap(): lax.ppermute(value, 'tp', [(source, source ^ bit) for source in range(cou...  16.7 us
    ppermute x4, waiting for transfers between devices, crossed(): return lax.ppermute(rows, 'h', [(0, 1), (1, 0)])  12 us
    ppermute x3, waiting for transfers between devices, shards(): parts.append(lax.ppermute(part_own, 'r', pairs))  10.6 us
    pallas_call x2, Pallas kernels, hidden_rows(): pl.pallas_call(lambda *refs: hidden_kernel(places, blocks, *refs), out_sh...  8.19 us
  transfers between devices with their start and end apart: 63, of which 21 were waited for; matrix products, arithmetic and copies ran while one was open for 2% of the time, Pallas kernels for 14%

profile of v1, /device:TPU:0, one launch (start us, length us, event | category | flops | bytes accessed | tf_op | source)
XLA Modules:
  0.0 207.6 jit_solution(10944377244299624798)
XLA Ops:
  2.1 2.6 %collective-permute-start.5 = (f32[35,256]{1,0:T(8,128)S(1)}, f32[35,256]{1,0:T(8,128)S(1)}, u32[]{:S(2)}, u32[]{:S(2)}) collective-permute-start(f32[35,256]{1,0:T(8,128)S(1)} %pad_maximum_fusion.2.refs_4_), channel_id=1, source_target_pairs={{0,2},{1,3},{2,0},{3,1},{4,6},{5,7},{6,4},{7,5},{8,10},{9,11},{10,... | collective-permute-start | bytes 107528 | tf_op jit(solution)/shard_map/ppermute | solution.py:20
  5.9 3.4 %collective-permute-start = (bf16[32,256]{1,0:T(8,128)(2,1)S(1)}, bf16[32,256]{1,0:T(8,128)(2,1)S(1)}, u32[]{:S(2)}, u32[]{:S(2)}) collective-permute-start(bf16[32,256]{1,0:T(8,128)(2,1)S(1)} %slice.36), channel_id=1, source_target_pairs={{0,4},{4,8},{8,12},{12,16},{16,20},{20,24},{24,28},{1,5},{5,9},{9,... | collective-permute-start | bytes 49160 | tf_op jit(solution)/shard_map/ppermute | solution.py:506
  12.3 2.7 %collective-permute-start.22 = (f32[4,128]{1,0:T(4,128)S(1)}, f32[4,128]{1,0:T(4,128)S(1)}, u32[]{:S(2)}, u32[]{:S(2)}) collective-permute-start(f32[4,128]{1,0:T(4,128)S(1)} %pad_maximum_fusion.3.refs_1_), channel_id=1, source_target_pairs={{0,16},{16,0},{1,17},{17,1},{2,18},{18,2},{3,19},{19,3},{4,20},{20... | collective-permute-start | bytes 6152 | tf_op jit(solution)/shard_map/ppermute | solution.py:537
  17.1 1.3 collective-permute-start.6
  19.3 1.5 collective-permute-start.9
  20.9 1.6 collective-permute-start.17
  23.3 1.6 collective-permute-start.3
  25.0 5.7 %collective-permute-done.3.refs_3_ = bf16[160,256]{1,0:T(8,128)(2,1)S(1)} collective-permute-done((bf16[160,256]{1,0:T(8,128)(2,1)S(1)}, bf16[160,256]{1,0:T(8,128)(2,1)S(1)}, u32[]{:S(2)}, u32[]{:S(2)}) %collective-permute-start.3) | collective-permute-done | bytes 81952 | tf_op jit(solution)/shard_map/ppermute | solution.py:20
  33.6 1.2 collective-permute-start.10
  35.5 1.3 collective-permute-start.11
  36.8 6.0 %collective-permute-done.10.refs_6_ = bf16[64,2048]{1,0:T(8,128)(2,1)S(1)} collective-permute-done((bf16[64,2048]{1,0:T(8,128)(2,1)S(1)}, bf16[64,2048]{1,0:T(8,128)(2,1)S(1)}, u32[]{:S(2)}, u32[]{:S(2)}) %collective-permute-start.10) | collective-permute-done | bytes 262176 | tf_op jit(solution)/shard_map/ppermute | solution.py:487
  43.5 4.7 %collective-permute-done.11.refs_7_ = bf16[64,2048]{1,0:T(8,128)(2,1)S(1)} collective-permute-done((bf16[64,2048]{1,0:T(8,128)(2,1)S(1)}, bf16[64,2048]{1,0:T(8,128)(2,1)S(1)}, u32[]{:S(2)}, u32[]{:S(2)}) %collective-permute-start.11) | collective-permute-done | bytes 262176 | tf_op jit(solution)/shard_map/ppermute | solution.py:487
  58.4 16.1 %collective-permute-done.33.refs_1_ = bf16[2048,256]{1,0:T(8,128)(2,1)} collective-permute-done((bf16[2048,256]{1,0:T(8,128)(2,1)}, bf16[2048,256]{1,0:T(8,128)(2,1)}, u32[]{:S(2)}, u32[]{:S(2)}) %collective-permute-start.33) | collective-permute-done | bytes 1048608 | tf_op jit(solution)/shard_map/ppermute | solution.py:20
  79.6 2.9 %conv.1 = (bf16[128,1024]{1,0:T(8,128)(2,1)S(1)}, f32[8,256]{1,0:T(8,128)S(1)}) custom-call(bf16[160,256]{1,0:T(8,128)(2,1)S(1)} %get-tuple-element.120.refs_0_, bf16[160,256]{1,0:T(8,128)(2,1)S(1)} %copy-done.36, bf16[160,256]{1,0:T(8,128)(2,1)S(1)} %copy-done.38, bf16[160,256]{1,0:T(8,128)(2,1)S(1)} %copy-done.40, ...), custom_call_target="tpu_custom_call" | custom-call | flops 8126464 | bytes 655360 | tf_op jit(solution)/shard_map/conv/pallas_call | solution.py:315
  82.5 1.2 copy-done.4
  87.8 1.7 middle.1
  90.0 16.4 %collective-permute-done.38.refs_4_ = bf16[256,1024]{1,0:T(8,128)(2,1)S(1)} collective-permute-done((bf16[256,1024]{1,0:T(8,128)(2,1)S(1)}, bf16[256,1024]{1,0:T(8,128)(2,1)S(1)}, u32[]{:S(2)}, u32[]{:S(2)}) %collective-permute-start.38) | collective-permute-done | bytes 524320 | tf_op jit(solution)/shard_map/ppermute | solution.py:20
  107.3 2.4 %collective-permute-start.23 = (bf16[128,1024]{1,0:T(8,128)(2,1)S(1)}, bf16[128,1024]{1,0:T(8,128)(2,1)S(1)}, u32[]{:S(2)}, u32[]{:S(2)}) collective-permute-start(bf16[128,1024]{1,0:T(8,128)(2,1)S(1)} %get-tuple-element.58.refs_1_), channel_id=1, source_target_pairs={{0,16},{16,0},{1,17},{17,1},{2,18},{18,2},{3,19},{19,3},{4,20},{20... | collective-permute-start | bytes 786440 | tf_op jit(solution)/shard_map/ppermute | solution.py:564
  110.6 2.6 %collective-permute-done.19.refs_1_ = bf16[64,2048]{1,0:T(8,128)(2,1)S(1)} collective-permute-done((bf16[64,2048]{1,0:T(8,128)(2,1)S(1)}, bf16[64,2048]{1,0:T(8,128)(2,1)S(1)}, u32[]{:S(2)}, u32[]{:S(2)}) %collective-permute-start.19) | collective-permute-done | bytes 262176 | tf_op jit(solution)/shard_map/ppermute | solution.py:556
  113.2 2.5 %collective-permute-start.21 = (bf16[64,2048]{1,0:T(8,128)(2,1)S(1)}, bf16[64,2048]{1,0:T(8,128)(2,1)S(1)}, u32[]{:S(2)}, u32[]{:S(2)}) collective-permute-start(bf16[64,2048]{1,0:T(8,128)(2,1)S(1)} %get-tuple-element.63), channel_id=1, source_target_pairs={{0,12},{4,8},{8,4},{12,0},{1,13},{5,9},{9,5},{13,1},{2,14},{6,10},... | collective-permute-start | bytes 786440 | tf_op jit(solution)/shard_map/ppermute | solution.py:556
  115.7 7.0 %collective-permute-done.23.refs_1_ = bf16[128,1024]{1,0:T(8,128)(2,1)S(1)} collective-permute-done((bf16[128,1024]{1,0:T(8,128)(2,1)S(1)}, bf16[128,1024]{1,0:T(8,128)(2,1)S(1)}, u32[]{:S(2)}, u32[]{:S(2)}) %collective-permute-start.23) | collective-permute-done | bytes 262176 | tf_op jit(solution)/shard_map/ppermute | solution.py:564
  123.7 1.4 collective-permute-start.24
  125.1 6.9 %collective-permute-done.21.refs_3_ = bf16[64,2048]{1,0:T(8,128)(2,1)S(1)} collective-permute-done((bf16[64,2048]{1,0:T(8,128)(2,1)S(1)}, bf16[64,2048]{1,0:T(8,128)(2,1)S(1)}, u32[]{:S(2)}, u32[]{:S(2)}) %collective-permute-start.21) | collective-permute-done | bytes 262176 | tf_op jit(solution)/shard_map/ppermute | solution.py:556
  132.0 5.1 %collective-permute-done.27.refs_1_ = bf16[128,1024]{1,0:T(8,128)(2,1)S(1)} collective-permute-done((bf16[128,1024]{1,0:T(8,128)(2,1)S(1)}, bf16[128,1024]{1,0:T(8,128)(2,1)S(1)}, u32[]{:S(2)}, u32[]{:S(2)}) %collective-permute-start.27) | collective-permute-done | bytes 262176 | tf_op jit(solution)/shard_map/ppermute | solution.py:564
  138.8 2.1 %collective-permute-start.29 = (bf16[64,1024]{1,0:T(8,128)(2,1)S(1)}, bf16[64,1024]{1,0:T(8,128)(2,1)S(1)}, u32[]{:S(2)}, u32[]{:S(2)}) collective-permute-start(bf16[64,1024]{1,0:T(8,128)(2,1)S(1)} %get-tuple-element.71), channel_id=1, source_target_pairs={{0,8},{4,12},{8,0},{12,4},{1,9},{5,13},{9,1},{13,5},{2,10},{6,14},... | collective-permute-start | bytes 393224 | tf_op jit(solution)/shard_map/ppermute | solution.py:556
  140.9 2.8 %collective-permute-done.26.refs_7_ = bf16[64,1024]{1,0:T(8,128)(2,1)S(1)} collective-permute-done((bf16[64,1024]{1,0:T(8,128)(2,1)S(1)}, bf16[64,1024]{1,0:T(8,128)(2,1)S(1)}, u32[]{:S(2)}, u32[]{:S(2)}) %collective-permute-start.26) | collective-permute-done | bytes 131104 | tf_op jit(solution)/shard_map/ppermute | solution.py:556
  145.8 3.8 %collective-permute-done.30.refs_11_ = bf16[64,1024]{1,0:T(8,128)(2,1)S(1)} collective-permute-done((bf16[64,1024]{1,0:T(8,128)(2,1)S(1)}, bf16[64,1024]{1,0:T(8,128)(2,1)S(1)}, u32[]{:S(2)}, u32[]{:S(2)}) %collective-permute-start.30) | collective-permute-done | bytes 131104 | tf_op jit(solution)/shard_map/ppermute | solution.py:556
  150.1 4.1 %hid.2 = (bf16[256,512]{1,0:T(8,128)(2,1)S(1)}, bf16[256,512]{1,0:T(8,128)(2,1)S(1)}, bf16[512,2048]{1,0:T(8,128)(2,1)S(1)}) custom-call(bf16[64,2048]{1,0:T(8,128)(2,1)S(1)} %get-tuple-element.60.refs_0_, bf16[64,2048]{1,0:T(8,128)(2,1)S(1)} %collective-permute-done.19.refs_1_, bf16[64,2048]{1,0:T(8,128)(2,1)S(1)} %collective-permute-done.20.refs_2_, ...), custom_call_target="tpu_custom_call" | custom-call | flops 2147483648 | bytes 6815744 | tf_op jit(solution)/shard_map/hid/pallas_call | solution.py:94
  154.2 4.1 %hid.3 = (bf16[256,512]{1,0:T(8,128)(2,1)S(1)}, bf16[256,512]{1,0:T(8,128)(2,1)S(1)}) custom-call(bf16[512,2048]{1,0:T(8,128)(2,1)S(1)} %get-tuple-element.74.refs_0_, bf16[2048,256]{1,0:T(8,128)(2,1)} %collective-permute-done.33.refs_1_, bf16[2048,256]{1,0:T(8,128)(2,1)} %collective-permute-done.34.refs_2_, ...), custom_call_target="tpu_custom_call" | custom-call | flops 2147483648 | bytes 6815744 | tf_op jit(solution)/shard_map/hid/pallas_call | solution.py:94
  159.4 1.5 collective-permute-start.56
  160.9 2.1 collective-permute-start.58
  164.1 1.5 collective-permute-start.43
  165.6 2.1 collective-permute-start.45
  167.7 2.5 %collective-permute-done.58.refs_5_ = bf16[64,1024]{1,0:T(8,128)(2,1)S(1)} collective-permute-done((bf16[64,1024]{1,0:T(8,128)(2,1)S(1)}, bf16[64,1024]{1,0:T(8,128)(2,1)S(1)}, u32[]{:S(2)}, u32[]{:S(2)}) %collective-permute-start.58) | collective-permute-done | bytes 131104 | tf_op jit(solution)/shard_map/ppermute | solution.py:556
  170.2 1.7 weighted.6
  171.9 1.6 collective-permute-start.59
  173.5 1.8 down.6
  176.0 1.9 collective-permute-start.54
  179.9 1.4 collective-permute-start.46
  182.2 1.8 down.4
  184.7 1.4 collective-permute-start.40
  186.2 4.6 %collective-permute-done.55.refs_5_ = bf16[64,1024]{1,0:T(8,128)(2,1)} collective-permute-done((bf16[64,1024]{1,0:T(8,128)(2,1)}, bf16[64,1024]{1,0:T(8,128)(2,1)}, u32[]{:S(2)}, u32[]{:S(2)}) %collective-permute-start.55) | collective-permute-done | bytes 131104 | tf_op jit(solution)/shard_map/ppermute | solution.py:556
  191.7 1.7 weighted.7
  193.6 2.6 %collective-permute-done.41.refs_4_ = bf16[64,1024]{1,0:T(8,128)(2,1)S(1)} collective-permute-done((bf16[64,1024]{1,0:T(8,128)(2,1)}, bf16[64,1024]{1,0:T(8,128)(2,1)S(1)}, u32[]{:S(2)}, u32[]{:S(2)}) %collective-permute-start.41) | collective-permute-done | bytes 131104 | tf_op jit(solution)/shard_map/ppermute | solution.py:556
  196.3 2.2 %collective-permute-done.42.refs_5_ = bf16[64,1024]{1,0:T(8,128)(2,1)S(1)} collective-permute-done((bf16[64,1024]{1,0:T(8,128)(2,1)}, bf16[64,1024]{1,0:T(8,128)(2,1)S(1)}, u32[]{:S(2)}, u32[]{:S(2)}) %collective-permute-start.42) | collective-permute-done | bytes 131104 | tf_op jit(solution)/shard_map/ppermute | solution.py:556
  199.4 2.0 weighted.5
  201.5 1.2 collective-permute-start.48
  203.5 2.4 %collective-permute-done.47 = bf16[128,256]{1,0:T(8,128)(2,1)S(1)} collective-permute-done((bf16[128,256]{1,0:T(8,128)(2,1)S(1)}, bf16[128,256]{1,0:T(8,128)(2,1)S(1)}, u32[]{:S(2)}, u32[]{:S(2)}) %collective-permute-start.47) | collective-permute-done | bytes 65568 | tf_op jit(solution)/shard_map/ppermute | solution.py:20
  (214 shorter events, 52.7 us)
Async XLA Ops:
  1.6 17.2 %collective-permute-start.4 = (f32[35,256]{1,0:T(8,128)S(1)}, f32[35,256]{1,0:T(8,128)S(1)}, u32[]{:S(2)}, u32[]{:S(2)}) collective-permute-start(f32[35,256]{1,0:T(8,128)S(1)} %pad_maximum_fusion.2.refs_4_), channel_id=1, source_target_pairs={{0,1},{1,0},{2,3},{3,2},{4,5},{5,4},{6,7},{7,6},{8,9},{9,8},{10,11... | collective-permute-start | bytes 107528 | tf_op jit(solution)/shard_map/ppermute | solution.py:20
  2.1 18.8 %collective-permute-start.5 = (f32[35,256]{1,0:T(8,128)S(1)}, f32[35,256]{1,0:T(8,128)S(1)}, u32[]{:S(2)}, u32[]{:S(2)}) collective-permute-start(f32[35,256]{1,0:T(8,128)S(1)} %pad_maximum_fusion.2.refs_4_), channel_id=1, source_target_pairs={{0,2},{1,3},{2,0},{3,1},{4,6},{5,7},{6,4},{7,5},{8,10},{9,11},{10,... | collective-permute-start | bytes 107528 | tf_op jit(solution)/shard_map/ppermute | solution.py:20
  5.9 9.1 %collective-permute-start = (bf16[32,256]{1,0:T(8,128)(2,1)S(1)}, bf16[32,256]{1,0:T(8,128)(2,1)S(1)}, u32[]{:S(2)}, u32[]{:S(2)}) collective-permute-start(bf16[32,256]{1,0:T(8,128)(2,1)S(1)} %slice.36), channel_id=1, source_target_pairs={{0,4},{4,8},{8,12},{12,16},{16,20},{20,24},{24,28},{1,5},{5,9},{9,... | collective-permute-start | bytes 49160 | tf_op jit(solution)/shard_map/ppermute | solution.py:506
  10.3 9.0 %collective-permute-start.8 = (bf16[64,2048]{1,0:T(8,128)(2,1)S(1)}, bf16[64,2048]{1,0:T(8,128)(2,1)S(1)}, u32[]{:S(2)}, u32[]{:S(2)}) collective-permute-start(bf16[64,2048]{1,0:T(8,128)(2,1)S(1)} %constant_dynamic-slice_fusion.10), channel_id=1, source_target_pairs={{0,2},{1,3},{2,0},{3,1},{4,6},{5,7},{6,4},{7,5},{8,10},{9,11},{10,... | collective-permute-start | bytes 786440 | tf_op jit(solution)/shard_map/ppermute | solution.py:20
  18.4 13.4 %collective-permute-start.16 = (bf16[128,512]{1,0:T(8,128)(2,1)S(1)}, bf16[128,512]{1,0:T(8,128)(2,1)S(1)}, u32[]{:S(2)}, u32[]{:S(2)}) collective-permute-start(bf16[128,512]{1,0:T(8,128)(2,1)S(1)} %get-tuple-element.108), channel_id=1, source_target_pairs={{0,1},{1,0},{2,3},{3,2},{4,5},{5,4},{6,7},{7,6},{8,9},{9,8},{10,11... | collective-permute-start | bytes 393224 | tf_op jit(solution)/shard_map/ppermute | solution.py:20
  19.3 17.5 %collective-permute-start.9 = (bf16[64,2048]{1,0:T(8,128)(2,1)S(1)}, bf16[64,2048]{1,0:T(8,128)(2,1)S(1)}, u32[]{:S(2)}, u32[]{:S(2)}) collective-permute-start(bf16[64,2048]{1,0:T(8,128)(2,1)S(1)} %collective-permute-done.8.refs_4_), channel_id=1, source_target_pairs={{0,4},{4,0},{8,12},{12,8},{1,5},{5,1},{9,13},{13,9},{2,6},{6,2},{1... | collective-permute-start | bytes 786440 | tf_op jit(solution)/shard_map/ppermute | solution.py:487
  20.9 12.0 %collective-permute-start.17 = (bf16[128,512]{1,0:T(8,128)(2,1)S(1)}, bf16[128,512]{1,0:T(8,128)(2,1)S(1)}, u32[]{:S(2)}, u32[]{:S(2)}) collective-permute-start(bf16[128,512]{1,0:T(8,128)(2,1)S(1)} %get-tuple-element.110), channel_id=1, source_target_pairs={{0,2},{1,3},{2,0},{3,1},{4,6},{5,7},{6,4},{7,5},{8,10},{9,11},{10,... | collective-permute-start | bytes 393224 | tf_op jit(solution)/shard_map/ppermute | solution.py:20
  23.1 11.7 %collective-permute-start.18 = (bf16[128,512]{1,0:T(8,128)(2,1)S(1)}, bf16[128,512]{1,0:T(8,128)(2,1)S(1)}, u32[]{:S(2)}, u32[]{:S(2)}) collective-permute-start(bf16[128,512]{1,0:T(8,128)(2,1)S(1)} %get-tuple-element.107), channel_id=1, source_target_pairs={{0,3},{1,2},{2,1},{3,0},{4,7},{5,6},{6,5},{7,4},{8,11},{9,10},{10,... | collective-permute-start | bytes 393224 | tf_op jit(solution)/shard_map/ppermute | solution.py:20
  23.3 7.3 %collective-permute-start.3 = (bf16[160,256]{1,0:T(8,128)(2,1)S(1)}, bf16[160,256]{1,0:T(8,128)(2,1)S(1)}, u32[]{:S(2)}, u32[]{:S(2)}) collective-permute-start(bf16[160,256]{1,0:T(8,128)(2,1)S(1)} %get-tuple-element.119), channel_id=1, source_target_pairs={{0,3},{1,2},{2,1},{3,0},{4,7},{5,6},{6,5},{7,4},{8,11},{9,10},{10,... | collective-permute-start | bytes 245768 | tf_op jit(solution)/shard_map/ppermute | solution.py:20
  31.3 19.3 %collective-permute-start.51 = (bf16[256,1024]{1,0:T(8,128)(2,1)S(1)}, bf16[256,1024]{1,0:T(8,128)(2,1)S(1)}, u32[]{:S(2)}, u32[]{:S(2)}) collective-permute-start(bf16[256,1024]{1,0:T(8,128)(2,1)S(1)} %pad_maximum_fusion.1.refs_2_), channel_id=1, source_target_pairs={{0,2},{1,3},{2,0},{3,1},{4,6},{5,7},{6,4},{7,5},{8,10},{9,11},{10,... | collective-permute-start | bytes 1572872 | tf_op jit(solution)/shard_map/ppermute | solution.py:20
  32.5 23.1 %collective-permute-start.7 = (bf16[256,2048]{1,0:T(8,128)(2,1)S(1)}, bf16[256,2048]{1,0:T(8,128)(2,1)S(1)}, u32[]{:S(2)}, u32[]{:S(2)}) collective-permute-start(bf16[256,2048]{1,0:T(8,128)(2,1)S(1)} %copy-done), channel_id=1, source_target_pairs={{0,1},{1,0},{2,3},{3,2},{4,5},{5,4},{6,7},{7,6},{8,9},{9,8},{10,11... | collective-permute-start | bytes 3145736 | tf_op jit(solution)/shard_map/ppermute | solution.py:20
  33.6 9.2 %collective-permute-start.10 = (bf16[64,2048]{1,0:T(8,128)(2,1)S(1)}, bf16[64,2048]{1,0:T(8,128)(2,1)S(1)}, u32[]{:S(2)}, u32[]{:S(2)}) collective-permute-start(bf16[64,2048]{1,0:T(8,128)(2,1)S(1)} %collective-permute-done.8.refs_4_), channel_id=1, source_target_pairs={{0,8},{4,12},{8,0},{12,4},{1,9},{5,13},{9,1},{13,5},{2,10},{6,14},... | collective-permute-start | bytes 786440 | tf_op jit(solution)/shard_map/ppermute | solution.py:487
  35.5 12.7 %collective-permute-start.11 = (bf16[64,2048]{1,0:T(8,128)(2,1)S(1)}, bf16[64,2048]{1,0:T(8,128)(2,1)S(1)}, u32[]{:S(2)}, u32[]{:S(2)}) collective-permute-start(bf16[64,2048]{1,0:T(8,128)(2,1)S(1)} %collective-permute-done.8.refs_4_), channel_id=1, source_target_pairs={{0,12},{4,8},{8,4},{12,0},{1,13},{5,9},{9,5},{13,1},{2,14},{6,10},... | collective-permute-start | bytes 786440 | tf_op jit(solution)/shard_map/ppermute | solution.py:487
  36.8 12.3 %collective-permute-start.12 = (bf16[64,2048]{1,0:T(8,128)(2,1)S(1)}, bf16[64,2048]{1,0:T(8,128)(2,1)S(1)}, u32[]{:S(2)}, u32[]{:S(2)}) collective-permute-start(bf16[64,2048]{1,0:T(8,128)(2,1)S(1)} %collective-permute-done.8.refs_4_), channel_id=1, source_target_pairs={{0,1},{1,0},{2,3},{3,2},{4,5},{5,4},{6,7},{7,6},{8,9},{9,8},{10,11... | collective-permute-start | bytes 786440 | tf_op jit(solution)/shard_map/ppermute | solution.py:20
  42.8 9.1 %collective-permute-start.13 = (bf16[64,2048]{1,0:T(8,128)(2,1)S(1)}, bf16[64,2048]{1,0:T(8,128)(2,1)S(1)}, u32[]{:S(2)}, u32[]{:S(2)}) collective-permute-start(bf16[64,2048]{1,0:T(8,128)(2,1)S(1)} %collective-permute-done.9.refs_5_), channel_id=1, source_target_pairs={{0,1},{1,0},{2,3},{3,2},{4,5},{5,4},{6,7},{7,6},{8,9},{9,8},{10,11... | collective-permute-start | bytes 786440 | tf_op jit(solution)/shard_map/ppermute | solution.py:20
  48.1 26.3 %collective-permute-start.33 = (bf16[2048,256]{1,0:T(8,128)(2,1)}, bf16[2048,256]{1,0:T(8,128)(2,1)}, u32[]{:S(2)}, u32[]{:S(2)}) collective-permute-start(bf16[2048,256]{1,0:T(8,128)(2,1)} %bitcast.9.refs_12_), channel_id=1, source_target_pairs={{0,2},{1,3},{2,0},{3,1},{4,6},{5,7},{6,4},{7,5},{8,10},{9,11},{10,... | collective-permute-start | bytes 3145736 | tf_op jit(solution)/shard_map/ppermute | solution.py:20
  52.5 54.8 %collective-permute-start.34 = (bf16[2048,256]{1,0:T(8,128)(2,1)}, bf16[2048,256]{1,0:T(8,128)(2,1)}, u32[]{:S(2)}, u32[]{:S(2)}) collective-permute-start(bf16[2048,256]{1,0:T(8,128)(2,1)} %bitcast.10.refs_13_), channel_id=1, source_target_pairs={{0,2},{1,3},{2,0},{3,1},{4,6},{5,7},{6,4},{7,5},{8,10},{9,11},{10,... | collective-permute-start | bytes 3145736 | tf_op jit(solution)/shard_map/ppermute | solution.py:20
  54.3 53.0 %collective-permute-start.31 = (bf16[2048,256]{1,0:T(8,128)(2,1)}, bf16[2048,256]{1,0:T(8,128)(2,1)}, u32[]{:S(2)}, u32[]{:S(2)}) collective-permute-start(bf16[2048,256]{1,0:T(8,128)(2,1)} %bitcast.9.refs_12_), channel_id=1, source_target_pairs={{0,1},{1,0},{2,3},{3,2},{4,5},{5,4},{6,7},{7,6},{8,9},{9,8},{10,11... | collective-permute-start | bytes 3145736 | tf_op jit(solution)/shard_map/ppermute | solution.py:20
  55.0 54.7 %collective-permute-start.32 = (bf16[2048,256]{1,0:T(8,128)(2,1)}, bf16[2048,256]{1,0:T(8,128)(2,1)}, u32[]{:S(2)}, u32[]{:S(2)}) collective-permute-start(bf16[2048,256]{1,0:T(8,128)(2,1)} %bitcast.10.refs_13_), channel_id=1, source_target_pairs={{0,1},{1,0},{2,3},{3,2},{4,5},{5,4},{6,7},{7,6},{8,9},{9,8},{10,11... | collective-permute-start | bytes 3145736 | tf_op jit(solution)/shard_map/ppermute | solution.py:20
  56.6 49.9 %collective-permute-start.38 = (bf16[256,1024]{1,0:T(8,128)(2,1)S(1)}, bf16[256,1024]{1,0:T(8,128)(2,1)S(1)}, u32[]{:S(2)}, u32[]{:S(2)}) collective-permute-start(bf16[256,1024]{1,0:T(8,128)(2,1)S(1)} %pad_maximum_fusion.refs_2_), channel_id=1, source_target_pairs={{0,2},{1,3},{2,0},{3,1},{4,6},{5,7},{6,4},{7,5},{8,10},{9,11},{10,... | collective-permute-start | bytes 1572872 | tf_op jit(solution)/shard_map/ppermute | solution.py:20
  74.5 75.1 %collective-permute-start.35 = (bf16[2048,256]{1,0:T(8,128)(2,1)}, bf16[2048,256]{1,0:T(8,128)(2,1)S(1)}, u32[]{:S(2)}, u32[]{:S(2)}) collective-permute-start(bf16[2048,256]{1,0:T(8,128)(2,1)} %collective-permute-done.33.refs_1_), channel_id=1, source_target_pairs={{0,1},{1,0},{2,3},{3,2},{4,5},{5,4},{6,7},{7,6},{8,9},{9,8},{10,11... | collective-permute-start | bytes 3145736 | tf_op jit(solution)/shard_map/ppermute | solution.py:20
  107.3 46.9 %collective-permute-start.36 = (bf16[2048,256]{1,0:T(8,128)(2,1)}, bf16[2048,256]{1,0:T(8,128)(2,1)S(1)}, u32[]{:S(2)}, u32[]{:S(2)}) collective-permute-start(bf16[2048,256]{1,0:T(8,128)(2,1)} %collective-permute-done.34.refs_2_), channel_id=1, source_target_pairs={{0,1},{1,0},{2,3},{3,2},{4,5},{5,4},{6,7},{7,6},{8,9},{9,8},{10,11... | collective-permute-start | bytes 3145736 | tf_op jit(solution)/shard_map/ppermute | solution.py:20
  107.3 15.3 %collective-permute-start.23 = (bf16[128,1024]{1,0:T(8,128)(2,1)S(1)}, bf16[128,1024]{1,0:T(8,128)(2,1)S(1)}, u32[]{:S(2)}, u32[]{:S(2)}) collective-permute-start(bf16[128,1024]{1,0:T(8,128)(2,1)S(1)} %get-tuple-element.58.refs_1_), channel_id=1, source_target_pairs={{0,16},{16,0},{1,17},{17,1},{2,18},{18,2},{3,19},{19,3},{4,20},{20... | collective-permute-start | bytes 786440 | tf_op jit(solution)/shard_map/ppermute | solution.py:564
  109.7 14.0 %collective-permute-start.20 = (bf16[64,2048]{1,0:T(8,128)(2,1)S(1)}, bf16[64,2048]{1,0:T(8,128)(2,1)S(1)}, u32[]{:S(2)}, u32[]{:S(2)}) collective-permute-start(bf16[64,2048]{1,0:T(8,128)(2,1)S(1)} %get-tuple-element.62), channel_id=1, source_target_pairs={{0,8},{4,12},{8,0},{12,4},{1,9},{5,13},{9,1},{13,5},{2,10},{6,14},... | collective-permute-start | bytes 786440 | tf_op jit(solution)/shard_map/ppermute | solution.py:556
  113.2 18.8 %collective-permute-start.21 = (bf16[64,2048]{1,0:T(8,128)(2,1)S(1)}, bf16[64,2048]{1,0:T(8,128)(2,1)S(1)}, u32[]{:S(2)}, u32[]{:S(2)}) collective-permute-start(bf16[64,2048]{1,0:T(8,128)(2,1)S(1)} %get-tuple-element.63), channel_id=1, source_target_pairs={{0,12},{4,8},{8,4},{12,0},{1,13},{5,9},{9,5},{13,1},{2,14},{6,10},... | collective-permute-start | bytes 786440 | tf_op jit(solution)/shard_map/ppermute | solution.py:556
  122.7 14.4 %collective-permute-start.27 = (bf16[128,1024]{1,0:T(8,128)(2,1)S(1)}, bf16[128,1024]{1,0:T(8,128)(2,1)S(1)}, u32[]{:S(2)}, u32[]{:S(2)}) collective-permute-start(bf16[128,1024]{1,0:T(8,128)(2,1)S(1)} %get-tuple-element.59.refs_2_), channel_id=1, source_target_pairs={{0,16},{16,0},{1,17},{17,1},{2,18},{18,2},{3,19},{19,3},{4,20},{20... | collective-permute-start | bytes 786440 | tf_op jit(solution)/shard_map/ppermute | solution.py:564
  123.7 13.9 %collective-permute-start.24 = (bf16[64,1024]{1,0:T(8,128)(2,1)S(1)}, bf16[64,1024]{1,0:T(8,128)(2,1)S(1)}, u32[]{:S(2)}, u32[]{:S(2)}) collective-permute-start(bf16[64,1024]{1,0:T(8,128)(2,1)S(1)} %get-tuple-element.66), channel_id=1, source_target_pairs={{0,4},{4,0},{8,12},{12,8},{1,5},{5,1},{9,13},{13,9},{2,6},{6,2},{1... | collective-permute-start | bytes 393224 | tf_op jit(solution)/shard_map/ppermute | solution.py:556
  137.7 7.1 %collective-permute-start.28 = (bf16[64,1024]{1,0:T(8,128)(2,1)S(1)}, bf16[64,1024]{1,0:T(8,128)(2,1)S(1)}, u32[]{:S(2)}, u32[]{:S(2)}) collective-permute-start(bf16[64,1024]{1,0:T(8,128)(2,1)S(1)} %get-tuple-element.70), channel_id=1, source_target_pairs={{0,4},{4,0},{8,12},{12,8},{1,5},{5,1},{9,13},{13,9},{2,6},{6,2},{1... | collective-permute-start | bytes 393224 | tf_op jit(solution)/shard_map/ppermute | solution.py:556
  138.8 7.0 %collective-permute-start.29 = (bf16[64,1024]{1,0:T(8,128)(2,1)S(1)}, bf16[64,1024]{1,0:T(8,128)(2,1)S(1)}, u32[]{:S(2)}, u32[]{:S(2)}) collective-permute-start(bf16[64,1024]{1,0:T(8,128)(2,1)S(1)} %get-tuple-element.71), channel_id=1, source_target_pairs={{0,8},{4,12},{8,0},{12,4},{1,9},{5,13},{9,1},{13,5},{2,10},{6,14},... | collective-permute-start | bytes 393224 | tf_op jit(solution)/shard_map/ppermute | solution.py:556
  144.8 13.5 %collective-permute-start.50 = (bf16[256,1024]{1,0:T(8,128)(2,1)S(1)}, bf16[256,1024]{1,0:T(8,128)(2,1)S(1)}, u32[]{:S(2)}, u32[]{:S(2)}) collective-permute-start(bf16[256,1024]{1,0:T(8,128)(2,1)S(1)} %pad_maximum_fusion.1.refs_2_), channel_id=1, source_target_pairs={{0,1},{1,0},{2,3},{3,2},{4,5},{5,4},{6,7},{7,6},{8,9},{9,8},{10,11... | collective-permute-start | bytes 1572872 | tf_op jit(solution)/shard_map/ppermute | solution.py:20
  145.8 12.5 %collective-permute-start.52 = (bf16[256,1024]{1,0:T(8,128)(2,1)S(1)}, bf16[256,1024]{1,0:T(8,128)(2,1)S(1)}, u32[]{:S(2)}, u32[]{:S(2)}) collective-permute-start(bf16[256,1024]{1,0:T(8,128)(2,1)S(1)} %collective-permute-done.51.refs_4_), channel_id=1, source_target_pairs={{0,1},{1,0},{2,3},{3,2},{4,5},{5,4},{6,7},{7,6},{8,9},{9,8},{10,11... | collective-permute-start | bytes 1572872 | tf_op jit(solution)/shard_map/ppermute | solution.py:20
  149.6 13.4 %collective-permute-start.37 = (bf16[256,1024]{1,0:T(8,128)(2,1)S(1)}, bf16[256,1024]{1,0:T(8,128)(2,1)S(1)}, u32[]{:S(2)}, u32[]{:S(2)}) collective-permute-start(bf16[256,1024]{1,0:T(8,128)(2,1)S(1)} %pad_maximum_fusion.refs_2_), channel_id=1, source_target_pairs={{0,1},{1,0},{2,3},{3,2},{4,5},{5,4},{6,7},{7,6},{8,9},{9,8},{10,11... | collective-permute-start | bytes 1572872 | tf_op jit(solution)/shard_map/ppermute | solution.py:20
  149.6 13.4 %collective-permute-start.39 = (bf16[256,1024]{1,0:T(8,128)(2,1)S(1)}, bf16[256,1024]{1,0:T(8,128)(2,1)S(1)}, u32[]{:S(2)}, u32[]{:S(2)}) collective-permute-start(bf16[256,1024]{1,0:T(8,128)(2,1)S(1)} %collective-permute-done.38.refs_4_), channel_id=1, source_target_pairs={{0,1},{1,0},{2,3},{3,2},{4,5},{5,4},{6,7},{7,6},{8,9},{9,8},{10,11... | collective-permute-start | bytes 1572872 | tf_op jit(solution)/shard_map/ppermute | solution.py:20
  160.9 9.2 %collective-permute-start.58 = (bf16[64,1024]{1,0:T(8,128)(2,1)S(1)}, bf16[64,1024]{1,0:T(8,128)(2,1)S(1)}, u32[]{:S(2)}, u32[]{:S(2)}) collective-permute-start(bf16[64,1024]{1,0:T(8,128)(2,1)S(1)} %get-tuple-element.98), channel_id=1, source_target_pairs={{0,12},{4,8},{8,4},{12,0},{1,13},{5,9},{9,5},{13,1},{2,14},{6,10},... | collective-permute-start | bytes 393224 | tf_op jit(solution)/shard_map/ppermute | solution.py:556
  164.1 11.9 %collective-permute-start.43 = (bf16[64,1024]{1,0:T(8,128)(2,1)S(1)}, bf16[64,1024]{1,0:T(8,128)(2,1)S(1)}, u32[]{:S(2)}, u32[]{:S(2)}) collective-permute-start(bf16[64,1024]{1,0:T(8,128)(2,1)S(1)} %get-tuple-element.87), channel_id=1, source_target_pairs={{0,4},{4,0},{8,12},{12,8},{1,5},{5,1},{9,13},{13,9},{2,6},{6,2},{1... | collective-permute-start | bytes 393224 | tf_op jit(solution)/shard_map/ppermute | solution.py:556
  165.6 12.3 %collective-permute-start.44 = (bf16[64,1024]{1,0:T(8,128)(2,1)S(1)}, bf16[64,1024]{1,0:T(8,128)(2,1)S(1)}, u32[]{:S(2)}, u32[]{:S(2)}) collective-permute-start(bf16[64,1024]{1,0:T(8,128)(2,1)S(1)} %get-tuple-element.88), channel_id=1, source_target_pairs={{0,8},{4,12},{8,0},{12,4},{1,9},{5,13},{9,1},{13,5},{2,10},{6,14},... | collective-permute-start | bytes 393224 | tf_op jit(solution)/shard_map/ppermute | solution.py:556
  165.6 13.2 %collective-permute-start.45 = (bf16[64,1024]{1,0:T(8,128)(2,1)S(1)}, bf16[64,1024]{1,0:T(8,128)(2,1)S(1)}, u32[]{:S(2)}, u32[]{:S(2)}) collective-permute-start(bf16[64,1024]{1,0:T(8,128)(2,1)S(1)} %get-tuple-element.89), channel_id=1, source_target_pairs={{0,12},{4,8},{8,4},{12,0},{1,13},{5,9},{9,5},{13,1},{2,14},{6,10},... | collective-permute-start | bytes 393224 | tf_op jit(solution)/shard_map/ppermute | solution.py:556
  171.9 19.0 %collective-permute-start.59 = (bf16[128,1024]{1,0:T(8,128)(2,1)}, bf16[128,1024]{1,0:T(8,128)(2,1)}, u32[]{:S(2)}, u32[]{:S(2)}) collective-permute-start(bf16[128,1024]{1,0:T(8,128)(2,1)} %weighted.6), channel_id=1, source_target_pairs={{0,16},{16,0},{1,17},{17,1},{2,18},{18,2},{3,19},{19,3},{4,20},{20... | collective-permute-start | bytes 786440 | tf_op jit(solution)/shard_map/ppermute | solution.py:564
  175.3 9.4 %collective-permute-start.53 = (bf16[64,1024]{1,0:T(8,128)(2,1)}, bf16[64,1024]{1,0:T(8,128)(2,1)}, u32[]{:S(2)}, u32[]{:S(2)}) collective-permute-start(bf16[64,1024]{1,0:T(8,128)(2,1)} %get-tuple-element.91), channel_id=1, source_target_pairs={{0,4},{4,0},{8,12},{12,8},{1,5},{5,1},{9,13},{13,9},{2,6},{6,2},{1... | collective-permute-start | bytes 393224 | tf_op jit(solution)/shard_map/ppermute | solution.py:556
  176.0 10.2 %collective-permute-start.54 = (bf16[64,1024]{1,0:T(8,128)(2,1)}, bf16[64,1024]{1,0:T(8,128)(2,1)}, u32[]{:S(2)}, u32[]{:S(2)}) collective-permute-start(bf16[64,1024]{1,0:T(8,128)(2,1)} %get-tuple-element.92), channel_id=1, source_target_pairs={{0,8},{4,12},{8,0},{12,4},{1,9},{5,13},{9,1},{13,5},{2,10},{6,14},... | collective-permute-start | bytes 393224 | tf_op jit(solution)/shard_map/ppermute | solution.py:556
  178.0 12.9 %collective-permute-start.55 = (bf16[64,1024]{1,0:T(8,128)(2,1)}, bf16[64,1024]{1,0:T(8,128)(2,1)}, u32[]{:S(2)}, u32[]{:S(2)}) collective-permute-start(bf16[64,1024]{1,0:T(8,128)(2,1)} %get-tuple-element.93), channel_id=1, source_target_pairs={{0,12},{4,8},{8,4},{12,0},{1,13},{5,9},{9,5},{13,1},{2,14},{6,10},... | collective-permute-start | bytes 393224 | tf_op jit(solution)/shard_map/ppermute | solution.py:556
  179.9 18.6 %collective-permute-start.46 = (bf16[128,1024]{1,0:T(8,128)(2,1)S(1)}, bf16[128,1024]{1,0:T(8,128)(2,1)}, u32[]{:S(2)}, u32[]{:S(2)}) collective-permute-start(bf16[128,1024]{1,0:T(8,128)(2,1)S(1)} %weighted.4), channel_id=1, source_target_pairs={{0,16},{16,0},{1,17},{17,1},{2,18},{18,2},{3,19},{19,3},{4,20},{20... | collective-permute-start | bytes 786440 | tf_op jit(solution)/shard_map/ppermute | solution.py:564
  184.7 8.9 %collective-permute-start.40 = (bf16[64,1024]{1,0:T(8,128)(2,1)}, bf16[64,1024]{1,0:T(8,128)(2,1)S(1)}, u32[]{:S(2)}, u32[]{:S(2)}) collective-permute-start(bf16[64,1024]{1,0:T(8,128)(2,1)} %get-tuple-element.78), channel_id=1, source_target_pairs={{0,4},{4,0},{8,12},{12,8},{1,5},{5,1},{9,13},{13,9},{2,6},{6,2},{1... | collective-permute-start | bytes 393224 | tf_op jit(solution)/shard_map/ppermute | solution.py:556
  186.2 10.1 %collective-permute-start.41 = (bf16[64,1024]{1,0:T(8,128)(2,1)}, bf16[64,1024]{1,0:T(8,128)(2,1)S(1)}, u32[]{:S(2)}, u32[]{:S(2)}) collective-permute-start(bf16[64,1024]{1,0:T(8,128)(2,1)} %get-tuple-element.79), channel_id=1, source_target_pairs={{0,8},{4,12},{8,0},{12,4},{1,9},{5,13},{9,1},{13,5},{2,10},{6,14},... | collective-permute-start | bytes 393224 | tf_op jit(solution)/shard_map/ppermute | solution.py:556
  190.8 7.6 %collective-permute-start.42 = (bf16[64,1024]{1,0:T(8,128)(2,1)}, bf16[64,1024]{1,0:T(8,128)(2,1)S(1)}, u32[]{:S(2)}, u32[]{:S(2)}) collective-permute-start(bf16[64,1024]{1,0:T(8,128)(2,1)} %get-tuple-element.80), channel_id=1, source_target_pairs={{0,12},{4,8},{8,4},{12,0},{1,13},{5,9},{9,5},{13,1},{2,14},{6,10},... | collective-permute-start | bytes 393224 | tf_op jit(solution)/shard_map/ppermute | solution.py:556
  193.5 9.3 %collective-permute-start.60 = (bf16[128,256]{1,0:T(8,128)(2,1)S(1)}, bf16[128,256]{1,0:T(8,128)(2,1)S(1)}, u32[]{:S(2)}, u32[]{:S(2)}) collective-permute-start(bf16[128,256]{1,0:T(8,128)(2,1)S(1)} %get-tuple-element.128), channel_id=1, source_target_pairs={{0,3},{1,2},{2,1},{3,0},{4,7},{5,6},{6,5},{7,4},{8,11},{9,10},{10,... | collective-permute-start | bytes 196616 | tf_op jit(solution)/shard_map/ppermute | solution.py:20
  193.6 9.8 %collective-permute-start.61 = (bf16[128,256]{1,0:T(8,128)(2,1)S(1)}, bf16[128,256]{1,0:T(8,128)(2,1)S(1)}, u32[]{:S(2)}, u32[]{:S(2)}) collective-permute-start(bf16[128,256]{1,0:T(8,128)(2,1)S(1)} %get-tuple-element.127), channel_id=1, source_target_pairs={{0,2},{1,3},{2,0},{3,1},{4,6},{5,7},{6,4},{7,5},{8,10},{9,11},{10,... | collective-permute-start | bytes 196616 | tf_op jit(solution)/shard_map/ppermute | solution.py:20
  196.3 7.1 %collective-permute-start.62 = (bf16[128,256]{1,0:T(8,128)(2,1)S(1)}, bf16[128,256]{1,0:T(8,128)(2,1)S(1)}, u32[]{:S(2)}, u32[]{:S(2)}) collective-permute-start(bf16[128,256]{1,0:T(8,128)(2,1)S(1)} %get-tuple-element.126), channel_id=1, source_target_pairs={{0,1},{1,0},{2,3},{3,2},{4,5},{5,4},{6,7},{7,6},{8,9},{9,8},{10,11... | collective-permute-start | bytes 196616 | tf_op jit(solution)/shard_map/ppermute | solution.py:20
  (64 other events, 410.3 us)
